TPU v7x, 32 devices: a whole 2x2x4 slice. The times are simulated.
32 devices in a mesh: sp: 4 (over z), tp: 4 (over y, x), dp: 2 (over core).
Axes of the slice: x: 2, y: 2, z: 4, core: 2. Of those that a mesh axis runs over, the one named last changes fastest.
Arguments:
- latent: bfloat16 [2, 1536, 2048], P('dp', 'sp'), may hold values from -6 to 6
- conditioning: bfloat16 [2, 2048], P(None, 'sp'), may hold values from -6 to 6
- context_cond: bfloat16 [2048], P('sp'), may hold values from -6 to 6
- modulation: bfloat16 [3, 2048, 2048], P(None, 'sp', ('tp', 'dp')), may hold values from -4.2426407 to 4.2426407
- context: bfloat16 [2, 256, 2048], P('dp', 'sp'), may hold values from -6 to 6
- query_weight: bfloat16 [2048, 1024], P(None, 'tp'), may hold values from -2.1213203 to 2.1213203
- key_projection: bfloat16 [2048, 256], P(None, 'tp'), may hold values from -0.13258252 to 0.13258252
- value_projection: bfloat16 [2048, 256], P(None, 'tp'), may hold values from -0.125 to 0.125
- out_weight: bfloat16 [1024, 2048], P(None, 'tp'), may hold values from -0.1875 to 0.1875
- sink_head_logit: float32 [16], P('tp'), may hold values from 5 to 7.5
- prefix_logit_bias: float32 [16], P('tp'), may hold values from -2.5 to -1
Outputs:
- updated: float32 [2, 1536, 2048], P('dp', 'sp', 'tp')
All inputs are finite; a program needn't handle non-finite values.
Results may differ from a plain program's by a relative error of at most 0.0073.
Values may be sent and summed in bfloat16 or wider, within the bound.
A program may use at most 64 MiB of HBM per device.

v0:
```python
import functools

import jax
import jax.numpy as jnp
import numpy as np
from jax import lax
from jax.experimental import pallas as pl
from jax.experimental.pallas import tpu as pltpu
from jax.sharding import PartitionSpec as P

HEAD_SIZE = 64
GRID_W = 64
WINDOW_REACH = 128
NORM_EPSILON = 1e-06
ROTARY_BASE = 10000.0
MASKED = -1e30
LANES = 128
MESH = pl.DeviceIdType.MESH
F32 = jnp.float32
BF16 = jnp.bfloat16


def rotary_tables(grid_rows):
    half = HEAD_SIZE // 2
    quarter = half // 2
    lane = np.arange(LANES) % HEAD_SIZE
    frequency = ROTARY_BASE ** (-2.0 * (lane % quarter) / half)
    frequency = frequency.astype(np.float32).astype(np.float64)
    sign = np.where(lane % half < quarter, -1.0, 1.0)
    by_row = lane < half

    def tables(count, keep):
        angles = np.arange(count)[:, None] * frequency[None, :]
        cosine = np.where(keep[None, :], np.cos(angles), 0.0)
        sine = np.where(keep[None, :], np.sin(angles) * sign[None, :], 0.0)
        return np.stack([cosine, sine]).astype(np.float32)

    return tables(grid_rows, by_row), tables(GRID_W, ~by_row)


def block_kernel(
    dims,
    lat_hbm, cond_hbm, cctx_hbm, mod_hbm, ctx_hbm, qw_hbm, kw_hbm, vw_hbm, ow_hbm,
    sink_hbm, bias_hbm, rowt_hbm, colt_hbm,
    out_hbm,
    lat, cond, cctx, mod, ctx, qw, ow, sink, bias, rowt, colt,
    act, pack, packs, total, sendb, slots, modv,
    xn, xnc, nrm, nrmc, kvw, cosv, sinv, kvb, cxb, ke, ko, ve, vo, q, att, outv,
    in_sem, out_sem, a_s, a_r, b_s, b_r, h_s, h_r, c_s, c_r, g_s, g_r,
):
    n_sp, n_tp, n_dp, samples = dims
    sp, tp, dp = lax.axis_index("sp"), lax.axis_index("tp"), lax.axis_index("dp")
    n_td = n_tp * n_dp
    me = tp * n_dp + dp
    tok, width = lat.shape
    cols = mod.shape[2]
    n_ctx = ctx.shape[0]
    reach = WINDOW_REACH
    blocks = tok // reach
    q_width = qw.shape[1]
    pairs = q_width // LANES

    barrier = pltpu.get_barrier_semaphore()
    for o in range(1, n_sp):
        pl.semaphore_signal(
            barrier, inc=1, device_id={"sp": lax.rem(sp + o, n_sp)}, device_id_type=MESH
        )

    def td_peer(o):
        lin = lax.rem(me + o, n_td)
        return lin // n_dp, lax.rem(lin, n_dp)

    for o in range(1, n_td):
        t, d = td_peer(o)
        pl.semaphore_signal(barrier, inc=1, device_id={"tp": t, "dp": d}, device_id_type=MESH)

    pairs_in = [
        (cond_hbm, cond), (cctx_hbm, cctx), (mod_hbm, mod), (ctx_hbm, ctx), (lat_hbm, lat),
        (kw_hbm, kvw.at[pl.ds(0, HEAD_SIZE)]), (vw_hbm, kvw.at[pl.ds(HEAD_SIZE, HEAD_SIZE)]), (rowt_hbm, rowt), (colt_hbm, colt), (qw_hbm, qw),
        (sink_hbm, sink), (bias_hbm, bias), (ow_hbm, ow),
    ]
    loads = [
        pltpu.make_async_copy(src, dst, in_sem.at[i]) for i, (src, dst) in enumerate(pairs_in)
    ]
    for load in loads:
        load.start()

    act[...] = jnp.zeros_like(act)
    loads[0].wait()
    loads[1].wait()
    act[0:samples, :] = cond[...].astype(F32)
    act[samples : samples + 1, :] = cctx[...].astype(F32).reshape(1, cctx.shape[0])
    v = act[...]
    activated = (v / (1.0 + jnp.exp(-v))).astype(BF16)
    pack[...] = jnp.zeros_like(pack)
    loads[2].wait()
    n_rows = samples + 1
    for m in range(3):
        count = n_rows if m < 2 else samples
        part = jnp.dot(activated, mod[m], preferred_element_type=F32)
        pack[m * n_rows : m * n_rows + count, :] = part[0:count, :]

    pl.semaphore_wait(barrier, n_sp - 1 + n_td - 1)
    a_copies = []
    for o in range(1, n_sp):
        copy = pltpu.make_async_remote_copy(
            src_ref=pack, dst_ref=packs.at[o - 1], send_sem=a_s.at[o - 1], recv_sem=a_r.at[o - 1],
            device_id={"sp": lax.rem(sp + o, n_sp)}, device_id_type=MESH,
        )
        copy.start()
        a_copies.append(copy)

    step = 16
    chunk = 64

    def normalise(src, dst, first, last):
        def body(i, carry):
            rows = pl.ds(pl.multiple_of(i * chunk, chunk), chunk)
            x = src[rows, :].astype(F32)
            x = x - jnp.mean(x, axis=-1, keepdims=True)
            spread = jnp.mean(x * x, axis=-1, keepdims=True)
            dst[rows, :] = x * lax.rsqrt(spread + NORM_EPSILON)
            return carry

        lax.fori_loop(first, last, body, 0)

    loads[3].wait()
    normalise(ctx, xnc, 0, n_ctx // chunk)
    loads[4].wait()
    middle = tok // chunk // 3
    normalise(lat, xn, 0, middle)

    for copy in a_copies:
        copy.wait_recv()
    summed = pack[...]
    for o in range(1, n_sp):
        summed = summed + packs[o - 1]
    total[...] = summed
    for d in range(n_dp):
        for row, source in enumerate(
            (d, n_rows + d, 2 * n_rows + d, samples, n_rows + samples)
        ):
            sendb[d, row : row + 1, :] = total[source : source + 1, :]
        sendb[d, 5:8, :] = jnp.zeros((3, cols), F32)
    b_copies = []
    for o in range(1, n_td):
        t, d = td_peer(o)
        copy = pltpu.make_async_remote_copy(
            src_ref=sendb.at[d], dst_ref=slots.at[me], send_sem=b_s.at[o - 1],
            recv_sem=b_r.at[o - 1], device_id={"tp": t, "dp": d}, device_id_type=MESH,
        )
        copy.start()
        b_copies.append(copy)
    slots[me] = sendb[dp]

    normalise(lat, xn, middle, tok // chunk)
    loads[5].wait()
    loads[6].wait()
    loads[7].wait()
    loads[8].wait()
    groups = tok // GRID_W
    for g in range(groups):
        row = pl.ds(sp * groups + g, 1)
        span = slice(g * GRID_W, (g + 1) * GRID_W)
        cosv[span, :] = rowt[0, row, :] + colt[0]
        sinv[span, :] = rowt[1, row, :] + colt[1]
    loads[9].wait()
    loads[10].wait()
    loads[11].wait()

    for copy in b_copies:
        copy.wait_recv()
    for j in range(n_td):
        modv[:, j * cols : (j + 1) * cols] = slots[j]

    def condition(src, dst, count, shift_row, scale_row):
        def body(i, carry):
            rows = pl.ds(pl.multiple_of(i * step, step), step)
            scale = 1.0 + modv[scale_row : scale_row + 1, :]
            dst[rows, :] = (src[rows, :] * scale + modv[shift_row : shift_row + 1, :]).astype(BF16)
            return carry

        lax.fori_loop(0, count // step, body, 0)

    condition(xnc, nrmc, n_ctx, 3, 4)
    nt = (((1,), (1,)), ((), ()))
    cxb[0] = lax.dot_general(nrmc[...], kvw[...], nt, preferred_element_type=F32).astype(BF16)
    c_copies = []
    for o in range(1, n_sp):
        copy = pltpu.make_async_remote_copy(
            src_ref=cxb.at[0], dst_ref=cxb.at[o], send_sem=c_s.at[o - 1], recv_sem=c_r.at[o - 1],
            device_id={"sp": lax.rem(sp + o, n_sp)}, device_id_type=MESH,
        )
        copy.start()
        c_copies.append(copy)

    half = HEAD_SIZE // 2
    quarter = half // 2

    def turn(u, cosine, sine):
        w = u.shape[1]
        lane = lax.broadcasted_iota(jnp.int32, u.shape, 1)
        first = lax.rem(lane, half) < quarter
        swapped = jnp.where(first, pltpu.roll(u, w - quarter, 1), pltpu.roll(u, quarter, 1))
        return u * cosine + swapped * sine

    condition(xn, nrm, tok, 0, 1)
    u = lax.dot_general(nrm[...], kvw[...], nt, preferred_element_type=F32)
    key_lane = lax.broadcasted_iota(jnp.int32, u.shape, 1) < HEAD_SIZE
    kv_rows = jnp.where(key_lane, turn(u, cosv[...], sinv[...]), u)
    kvb[reach : reach + tok, :] = kv_rows.astype(BF16)

    up = pltpu.make_async_remote_copy(
        src_ref=kvb.at[pl.ds(tok, reach)], dst_ref=kvb.at[pl.ds(0, reach)],
        send_sem=h_s.at[0], recv_sem=h_r.at[0],
        device_id={"sp": lax.rem(sp + 1, n_sp)}, device_id_type=MESH,
    )
    down = pltpu.make_async_remote_copy(
        src_ref=kvb.at[pl.ds(reach, reach)], dst_ref=kvb.at[pl.ds(reach + tok, reach)],
        send_sem=h_s.at[1], recv_sem=h_r.at[1],
        device_id={"sp": lax.rem(sp + n_sp - 1, n_sp)}, device_id_type=MESH,
    )

    @pl.when(sp < n_sp - 1)
    def _():
        up.start()

    @pl.when(sp > 0)
    def _():
        down.start()

    factor = HEAD_SIZE ** (-0.5)
    u = jnp.dot(nrm[...], qw[...], preferred_element_type=F32)
    for p in range(pairs):
        span = slice(p * LANES, (p + 1) * LANES)
        q[:, span] = (turn(u[:, span], cosv[...], sinv[...]) * factor).astype(BF16)

    def expand(rows, at):
        x = rows.astype(F32)
        low = lax.broadcasted_iota(jnp.int32, x.shape, 1) < HEAD_SIZE
        keys = jnp.where(low, x, 0.0)
        vals = jnp.where(low, 0.0, x)
        span = slice(at, at + x.shape[0])
        ke[span, :] = keys.astype(BF16)
        ko[span, :] = pltpu.roll(keys, HEAD_SIZE, 1).astype(BF16)
        vo[span, :] = vals.astype(BF16)
        ve[span, :] = pltpu.roll(vals, HEAD_SIZE, 1).astype(BF16)

    window = tok + 2 * reach
    expand(kvb[reach : reach + tok, :], reach)
    expand(cxb[0], window)
    for o in range(1, n_sp):
        c_copies[o - 1].wait_recv()
        expand(cxb[o], window + o * n_ctx)

    m_rows = pairs * reach
    row = lax.broadcasted_iota(jnp.int32, (m_rows, 1), 0)

    def per_head(ref, parity):
        column = jnp.full((m_rows, 1), ref[parity], F32)
        for p in range(1, pairs):
            column = jnp.where(row >= p * reach, ref[2 * p + parity], column)
        return column

    n_all_ctx = n_sp * n_ctx
    delta = lax.broadcasted_iota(jnp.int32, (m_rows, reach), 1) - lax.rem(
        lax.broadcasted_iota(jnp.int32, (m_rows, reach), 0), reach
    )
    far = 4 * reach
    low_edge = jnp.where(sp == 0, far, 0)
    high_edge = jnp.where(sp == n_sp - 1, -far, 0)
    g_copies = {}
    relayed = n_tp == 4
    direct = (1, 2) if relayed else range(1, n_tp)

    def partner(o):
        if not relayed:
            return lax.rem(tp + o, n_tp)
        x, y = lax.rem(tp, 2), tp // 2
        x = 1 - x if o % 2 else x
        y = 1 - y if o // 2 else y
        return 2 * y + x

    def owner(o):
        return partner(o) if relayed else lax.rem(tp + n_tp - o, n_tp)


    def attend(b):
        rows = slice(b * reach, (b + 1) * reach)
        q2 = jnp.concatenate(
            [q[rows, p * LANES : (p + 1) * LANES] for p in range(pairs)], axis=0
        )
        before_ok = delta >= (low_edge if b == 0 else 0)
        after_ok = delta <= (high_edge if b == blocks - 1 else 0)
        win = slice(b * reach, (b + 3) * reach)
        pre = slice(window, window + n_all_ctx)
        result = jnp.zeros((m_rows, LANES), F32)
        for parity, k_ref, v_ref in ((0, ke, ve), (1, ko, vo)):
            sw = lax.dot_general(q2, k_ref[win, :], nt, preferred_element_type=F32)
            s0 = jnp.where(before_ok, sw[:, 0:reach], MASKED)
            s1 = sw[:, reach : 2 * reach]
            s2 = jnp.where(after_ok, sw[:, 2 * reach : 3 * reach], MASKED)
            sc = lax.dot_general(q2, k_ref[pre, :], nt, preferred_element_type=F32)
            sc = sc + per_head(bias, parity)
            sunk = per_head(sink, parity)
            top = jnp.maximum(jnp.maximum(s0, s1), s2)
            for c in range(n_all_ctx // LANES):
                top = jnp.maximum(top, sc[:, c * LANES : (c + 1) * LANES])
            highest = jnp.maximum(jnp.max(top, axis=-1, keepdims=True), sunk)
            e0, e1, e2 = jnp.exp(s0 - highest), jnp.exp(s1 - highest), jnp.exp(s2 - highest)
            ec = jnp.exp(sc - highest)
            mass = e0 + e1 + e2
            for c in range(n_all_ctx // LANES):
                mass = mass + ec[:, c * LANES : (c + 1) * LANES]
            denominator = jnp.sum(mass, axis=-1, keepdims=True) + jnp.exp(sunk - highest)
            ew = jnp.concatenate([e0, e1, e2], axis=1).astype(BF16)
            weighed = jnp.dot(ew, v_ref[win, :], preferred_element_type=F32)
            weighed = weighed + jnp.dot(ec.astype(BF16), v_ref[pre, :], preferred_element_type=F32)
            result = result + weighed / denominator
        for p in range(pairs):
            att[0, b, :, p * LANES : (p + 1) * LANES] = result[
                p * reach : (p + 1) * reach, :
            ].astype(BF16)
        for o in direct:
            copy = pltpu.make_async_remote_copy(
                src_ref=att.at[0, b], dst_ref=att.at[o, b], send_sem=g_s.at[b, o - 1],
                recv_sem=g_r.at[b, o - 1], device_id={"tp": partner(o)}, device_id_type=MESH,
            )
            copy.start()
            g_copies[b, o] = copy

    def forward(b):
        for o in direct:
            g_copies[b, o].wait_recv()
            part = pl.ds((o - 1) * (reach // 2), reach // 2)
            copy = pltpu.make_async_remote_copy(
                src_ref=att.at[o, b, part], dst_ref=att.at[3, b, part],
                send_sem=g_s.at[b, 1 + o], recv_sem=g_r.at[b, 1 + o],
                device_id={"tp": partner(3 - o)}, device_id_type=MESH,
            )
            copy.start()
            g_copies[b, 2 + o] = copy

    order = list(range(1, blocks - 1)) + ([0, blocks - 1] if blocks > 1 else [0])
    for b in order:
        if b == 0:
            @pl.when(sp > 0)
            def _():
                up.wait_recv()

            @pl.when(sp == 0)
            def _():
                kvb[0:reach, :] = jnp.zeros((reach, LANES), BF16)

            expand(kvb[0:reach, :], 0)
        if b == blocks - 1:
            @pl.when(sp < n_sp - 1)
            def _():
                down.wait_recv()

            @pl.when(sp == n_sp - 1)
            def _():
                kvb[reach + tok : window, :] = jnp.zeros((reach, LANES), BF16)

            expand(kvb[reach + tok : window, :], reach + tok)
        attend(b)

    loads[12].wait()
    out_cols = ow.shape[1]
    mine = pl.ds(pl.multiple_of(tp * out_cols, out_cols), out_cols)
    gate = modv[2:3, mine]
    writes = []

    def project(b, o):
        w = ow[pl.ds(pl.multiple_of(owner(o) * q_width, q_width), q_width), :]
        return jnp.dot(att[o, b], w, preferred_element_type=F32)

    for b in order:
        if relayed:
            forward(b)
        outv[b * reach : (b + 1) * reach, :] = project(b, 0)
    for b in order:
        rows = slice(b * reach, (b + 1) * reach)
        mixed = outv[rows, :]
        for o in range(1, n_tp):
            if not relayed:
                g_copies[b, o].wait_recv()
            elif o == 3:
                g_copies[b, 3].wait_recv()
                g_copies[b, 4].wait_recv()
            mixed = mixed + project(b, o)
        outv[rows, :] = lat[rows, mine].astype(F32) + gate * mixed
        write = pltpu.make_async_copy(outv.at[rows], out_hbm.at[rows], out_sem.at[b])
        write.start()
        writes.append(write)

    for copy in a_copies + b_copies + c_copies + list(g_copies.values()):
        copy.wait_send()

    @pl.when(sp < n_sp - 1)
    def _():
        up.wait_send()

    @pl.when(sp > 0)
    def _():
        down.wait_send()

    for write in writes:
        write.wait()


def per_device(
    latent, conditioning, context_cond, modulation, context, query_weight, key_projection,
    value_projection, out_weight, sink_head_logit, prefix_logit_bias,
):
    n_sp, n_tp, n_dp = lax.axis_size("sp"), lax.axis_size("tp"), lax.axis_size("dp")
    samples = conditioning.shape[0]
    _, tok, width = latent.shape
    n_ctx = context.shape[1]
    depth, cols = modulation.shape[1:]
    q_width = query_weight.shape[1]
    heads = q_width // HEAD_SIZE
    out_cols = out_weight.shape[1]
    blocks = tok // WINDOW_REACH
    window = tok + 2 * WINDOW_REACH
    keys = window + n_sp * n_ctx
    n_td = n_tp * n_dp
    act_rows = -(-(samples + 1) // 8) * 8
    pack_rows = -(-(3 * samples + 2) // 8) * 8
    row_table, col_table = rotary_tables(n_sp * tok // GRID_W)
    vm = pltpu.VMEM
    dma = pltpu.SemaphoreType.DMA
    scratch = [
        vm((tok, width), BF16), vm((samples, depth), BF16), vm((depth,), BF16),
        vm((3, depth, cols), BF16), vm((n_ctx, width), BF16), vm((width, q_width), BF16),
        vm(out_weight.shape, BF16), pltpu.SMEM((heads,), F32), pltpu.SMEM((heads,), F32),
        vm(row_table.shape, F32), vm(col_table.shape, F32),
        vm((act_rows, depth), F32), vm((pack_rows, cols), F32),
        vm((n_sp - 1, pack_rows, cols), F32), vm((pack_rows, cols), F32),
        vm((n_dp, 8, cols), F32), vm((n_td, 8, cols), F32), vm((8, width), F32),
        vm((tok, width), F32), vm((n_ctx, width), F32), vm((tok, width), BF16),
        vm((n_ctx, width), BF16), vm((LANES, width), BF16), vm((tok, LANES), F32),
        vm((tok, LANES), F32), vm((window, LANES), BF16), vm((n_sp, n_ctx, LANES), BF16),
        vm((keys, LANES), BF16), vm((keys, LANES), BF16), vm((keys, LANES), BF16),
        vm((keys, LANES), BF16), vm((tok, q_width), BF16),
        vm((n_tp, blocks, WINDOW_REACH, q_width), BF16), vm((tok, out_cols), F32),
        dma((13,)), dma((blocks,)), dma((n_sp - 1,)), dma((n_sp - 1,)), dma((n_td - 1,)),
        dma((n_td - 1,)), dma((2,)), dma((2,)), dma((n_sp - 1,)), dma((n_sp - 1,)),
        dma((blocks, n_tp)), dma((blocks, n_tp)),
    ]
    anywhere = pl.BlockSpec(memory_space=pl.ANY)
    stays = pl.BlockSpec(memory_space=pltpu.HBM)
    out = pl.pallas_call(
        functools.partial(block_kernel, (n_sp, n_tp, n_dp, samples)),
        out_shape=jax.ShapeDtypeStruct((tok, out_cols), F32),
        in_specs=[stays] * 13,
        out_specs=anywhere,
        scratch_shapes=scratch,
        compiler_params=pltpu.CompilerParams(
            collective_id=0, has_side_effects=True, vmem_limit_bytes=66000000
        ),
        name="fused_block",
    )(
        latent[0], conditioning, context_cond, modulation, context[0], query_weight,
        key_projection.T, value_projection.T, out_weight, sink_head_logit, prefix_logit_bias,
        jnp.asarray(row_table), jnp.asarray(col_table),
    )
    return out[None]


def solution(mesh):
    placed = (
        P("dp", "sp", None),
        P(None, "sp"),
        P("sp"),
        P(None, "sp", ("tp", "dp")),
        P("dp", "sp", None),
        P(None, "tp"),
        P(None, "tp"),
        P(None, "tp"),
        P(None, "tp"),
        P("tp"),
        P("tp"),
    )
    return jax.shard_map(
        per_device, mesh=mesh, in_specs=placed, out_specs=P("dp", "sp", "tp"), check_vma=False
    )
```

profile of v0, /device:TPU:0, one launch (start us, length us, event | category | flops | bytes accessed | tf_op | source)
XLA Modules:
  0.0 31.0 jit_solution(6343120702358424058)
XLA Ops:
  0.0 29.0 %fused_block.1 = f32[384,512]{1,0:T(8,128)} custom-call(bf16[384,2048]{1,0:T(8,128)(2,1)} %bitcast.6, bf16[2,512]{1,0:T(2,128)(2,1)} %cond_hbm.1, bf16[512]{0:T(512)(128)(2,1)} %cctx_hbm.1, bf16[3,512,256]{2,1,0:T(8,128)(2,1)} %mod_hbm.1, bf16[64,2048]{1,0:T(8,128)(2,1)} %bitcast.7, bf16[2048,256]{1,0:T(8,128)(2,1)} %qw_hbm.1, bf16[64,2048]{1,0:T(8,128)(2,1)} %bitcast.8, ...), custom_call_target="tpu_custom_call" | custom-call | tf_op jit(solution)/shard_map/fused_block/pallas_call | solution.py:453
  29.0 2.1 %copy.15 = f32[1,384,512]{2,1,0:T(8,128)} copy(f32[1,384,512]{2,1,0:T(8,128)} %bitcast.5) | data formatting | bytes 1572864
where the time goes:
time: 31.2 us; the launch traced here: 31 us
  Pallas kernels  29 us (93%)
  local copies, waits for them, and re-layouts  2.06 us (7%)
    pallas_call x1, Pallas kernels, per_device(): pl.pallas_call(functools.partial(block_kernel, (n_sp, n_tp, n_dp, samples...  29 us
    unnamed x1, local copies, waits for them, and re-layouts  2.06 us

commit v1 on v0

--- a/solution.py
+++ b/solution.py
@@ -42,11 +42,11 @@
     dims,
     lat_hbm, cond_hbm, cctx_hbm, mod_hbm, ctx_hbm, qw_hbm, kw_hbm, vw_hbm, ow_hbm,
     sink_hbm, bias_hbm, rowt_hbm, colt_hbm,
-    out_hbm,
+    outv,
     lat, cond, cctx, mod, ctx, qw, ow, sink, bias, rowt, colt,
     act, pack, packs, total, sendb, slots, modv,
-    xn, xnc, nrm, nrmc, kvw, cosv, sinv, kvb, cxb, ke, ko, ve, vo, q, att, outv,
-    in_sem, out_sem, a_s, a_r, b_s, b_r, h_s, h_r, c_s, c_r, g_s, g_r,
+    xn, xnc, nrm, nrmc, kvw, cosv, sinv, kvb, cxb, ke, ko, ve, vo, q, att,
+    in_sem, a_s, a_r, b_s, b_r, h_s, h_r, c_s, c_r, g_s, g_r,
 ):
     n_sp, n_tp, n_dp, samples = dims
     sp, tp, dp = lax.axis_index("sp"), lax.axis_index("tp"), lax.axis_index("dp")
@@ -369,7 +369,6 @@
     out_cols = ow.shape[1]
     mine = pl.ds(pl.multiple_of(tp * out_cols, out_cols), out_cols)
     gate = modv[2:3, mine]
-    writes = []
 
     def project(b, o):
         w = ow[pl.ds(pl.multiple_of(owner(o) * q_width, q_width), q_width), :]
@@ -390,9 +389,6 @@
                 g_copies[b, 4].wait_recv()
             mixed = mixed + project(b, o)
         outv[rows, :] = lat[rows, mine].astype(F32) + gate * mixed
-        write = pltpu.make_async_copy(outv.at[rows], out_hbm.at[rows], out_sem.at[b])
-        write.start()
-        writes.append(write)
 
     for copy in a_copies + b_copies + c_copies + list(g_copies.values()):
         copy.wait_send()
@@ -404,9 +400,6 @@
     @pl.when(sp > 0)
     def _():
         down.wait_send()
-
-    for write in writes:
-        write.wait()
 
 
 def per_device(
@@ -443,8 +436,8 @@
         vm((tok, LANES), F32), vm((window, LANES), BF16), vm((n_sp, n_ctx, LANES), BF16),
         vm((keys, LANES), BF16), vm((keys, LANES), BF16), vm((keys, LANES), BF16),
         vm((keys, LANES), BF16), vm((tok, q_width), BF16),
-        vm((n_tp, blocks, WINDOW_REACH, q_width), BF16), vm((tok, out_cols), F32),
-        dma((13,)), dma((blocks,)), dma((n_sp - 1,)), dma((n_sp - 1,)), dma((n_td - 1,)),
+        vm((n_tp, blocks, WINDOW_REACH, q_width), BF16),
+        dma((13,)), dma((n_sp - 1,)), dma((n_sp - 1,)), dma((n_td - 1,)),
         dma((n_td - 1,)), dma((2,)), dma((2,)), dma((n_sp - 1,)), dma((n_sp - 1,)),
         dma((blocks, n_tp)), dma((blocks, n_tp)),
     ]
@@ -452,9 +445,9 @@
     stays = pl.BlockSpec(memory_space=pltpu.HBM)
     out = pl.pallas_call(
         functools.partial(block_kernel, (n_sp, n_tp, n_dp, samples)),
-        out_shape=jax.ShapeDtypeStruct((tok, out_cols), F32),
+        out_shape=pltpu.VMEM((tok, out_cols), F32),
         in_specs=[stays] * 13,
-        out_specs=anywhere,
+        out_specs=pl.BlockSpec(memory_space=pltpu.VMEM),
         scratch_shapes=scratch,
         compiler_params=pltpu.CompilerParams(
             collective_id=0, has_side_effects=True, vmem_limit_bytes=66000000

time: 31.2 us -> 29.3 us (0.939)
  local copies, waits for them, and re-layouts: 2.06 us -> 0.88 us
  Pallas kernels: 29 us -> 28.3 us
    unnamed x1, local copies, waits for them, and re-layouts: 2.06 us -> 0.88 us
    pallas_call x1, Pallas kernels: 29 us -> 28.3 us  [per_device(): pl.pallas_call(functools.partial(block_kernel, (n_sp, n_tp, n_dp, samples...]
where the time goes in v1:
time: 29.3 us; the launch traced here: 29.2 us
  Pallas kernels  28.3 us (97%)
  local copies, waits for them, and re-layouts  0.88 us (3%)
    pallas_call x1, Pallas kernels, per_device(): pl.pallas_call(functools.partial(block_kernel, (n_sp, n_tp, n_dp, samples...  28.3 us
    unnamed x1, local copies, waits for them, and re-layouts  0.88 us

profile of v1, /device:TPU:0, one launch (start us, length us, event | category | flops | bytes accessed | tf_op | source)
XLA Modules:
  0.0 29.2 jit_solution(2367136712336618144)
XLA Ops:
  0.0 28.3 %fused_block.1 = f32[384,512]{1,0:T(8,128)S(1)} custom-call(bf16[384,2048]{1,0:T(8,128)(2,1)} %bitcast.6, bf16[2,512]{1,0:T(2,128)(2,1)} %cond_hbm.1, bf16[512]{0:T(512)(128)(2,1)} %cctx_hbm.1, bf16[3,512,256]{2,1,0:T(8,128)(2,1)} %mod_hbm.1, bf16[64,2048]{1,0:T(8,128)(2,1)} %bitcast.7, bf16[2048,256]{1,0:T(8,128)(2,1)} %qw_hbm.1, bf16[64,2048]{1,0:T(8,128)(2,1)} %bitcast.8, ...), custom_call_target="tpu_custom_call" | custom-call | tf_op jit(solution)/shard_map/fused_block/pallas_call | solution.py:446
  28.3 0.9 %copy.15 = f32[1,384,512]{2,1,0:T(8,128)} copy(f32[1,384,512]{2,1,0:T(8,128)S(1)} %bitcast.5) | data formatting | bytes 1572864

commit v2 on v1

v2 whole, which is shorter than its diff:
```python
import functools

import jax
import jax.numpy as jnp
import numpy as np
from jax import lax
from jax.experimental import pallas as pl
from jax.experimental.pallas import tpu as pltpu
from jax.sharding import PartitionSpec as P

HEAD_SIZE = 64
GRID_W = 64
WINDOW_REACH = 128
NORM_EPSILON = 1e-06
ROTARY_BASE = 10000.0
MASKED = -1e30
LANES = 128
MESH = pl.DeviceIdType.MESH
F32 = jnp.float32
BF16 = jnp.bfloat16


def rotary_tables(grid_rows):
    half = HEAD_SIZE // 2
    quarter = half // 2
    lane = np.arange(LANES) % HEAD_SIZE
    frequency = ROTARY_BASE ** (-2.0 * (lane % quarter) / half)
    frequency = frequency.astype(np.float32).astype(np.float64)
    sign = np.where(lane % half < quarter, -1.0, 1.0)
    by_row = lane < half

    def tables(count, keep):
        angles = np.arange(count)[:, None] * frequency[None, :]
        cosine = np.where(keep[None, :], np.cos(angles), 0.0)
        sine = np.where(keep[None, :], np.sin(angles) * sign[None, :], 0.0)
        return np.stack([cosine, sine]).astype(np.float32)

    return tables(grid_rows, by_row), tables(GRID_W, ~by_row)


def block_kernel(
    dims,
    lat_hbm, cond_hbm, cctx_hbm, mod_hbm, ctx_hbm, qw_hbm, kw_hbm, vw_hbm, ow_hbm,
    sink_hbm, bias_hbm, rowt_hbm, colt_hbm,
    outv,
    lat, cond, cctx, mod, ctx, wall, ow, sink, bias, rowt, colt,
    act, packf, pack, packs, total, sendb, slots, modv,
    xn, xnc, nrm, nrmc, kvw, cosv, sinv, acc, accc, kvb, cxb, kd, vd, q4, att,
    in_sem, a_s, a_r, b_s, b_r, h_s, h_r, c_s, c_r, g_s, g_r,
):
    n_sp, n_tp, n_dp, samples = dims
    sp, tp, dp = lax.axis_index("sp"), lax.axis_index("tp"), lax.axis_index("dp")
    n_td = n_tp * n_dp
    me = tp * n_dp + dp
    tok, width = lat.shape
    cols = mod.shape[2]
    group = n_dp * cols
    n_ctx = ctx.shape[0]
    reach = WINDOW_REACH
    blocks = tok // reach
    q_width = wall.shape[1] - LANES
    pairs = q_width // LANES
    heads = 2 * pairs

    barrier = pltpu.get_barrier_semaphore()
    for o in range(1, n_sp):
        pl.semaphore_signal(
            barrier, inc=1, device_id={"sp": lax.rem(sp + o, n_sp)}, device_id_type=MESH
        )
    for o in range(1, n_td):
        lin = lax.rem(me + o, n_td)
        pl.semaphore_signal(
            barrier, inc=1, device_id={"tp": lin // n_dp, "dp": lax.rem(lin, n_dp)},
            device_id_type=MESH,
        )

    relayed = n_tp == 4
    direct = (1, 2) if relayed else range(1, n_tp)

    def partner(o):
        if not relayed:
            return lax.rem(tp + o, n_tp)
        x, y = lax.rem(tp, 2), tp // 2
        x = 1 - x if o % 2 else x
        y = 1 - y if o // 2 else y
        return 2 * y + x

    def owner(o):
        return partner(o) if relayed else lax.rem(tp + n_tp - o, n_tp)

    pairs_in = [
        (cond_hbm, cond), (cctx_hbm, cctx), (mod_hbm.at[0], mod.at[0]), (mod_hbm.at[1], mod.at[1]),
        (mod_hbm.at[2], mod.at[2]), (ctx_hbm, ctx), (lat_hbm, lat),
        (kw_hbm, kvw.at[pl.ds(0, HEAD_SIZE)]), (vw_hbm, kvw.at[pl.ds(HEAD_SIZE, HEAD_SIZE)]),
        (rowt_hbm, rowt), (colt_hbm, colt), (qw_hbm, wall.at[:, pl.ds(0, q_width)]),
        (sink_hbm, sink), (bias_hbm, bias), (ow_hbm, ow),
    ]
    loads = [
        pltpu.make_async_copy(src, dst, in_sem.at[i]) for i, (src, dst) in enumerate(pairs_in)
    ]
    for load in loads[:6]:
        load.start()

    act[...] = jnp.zeros_like(act)
    loads[0].wait()
    loads[1].wait()
    for load in loads[6:]:
        load.start()
    act[0:samples, :] = cond[...].astype(F32)
    act[samples : samples + 1, :] = cctx[...].astype(F32).reshape(1, cctx.shape[0])
    v = act[...]
    activated = (v / (1.0 + jnp.exp(-v))).astype(BF16)
    packf[...] = jnp.zeros_like(packf)
    n_rows = samples + 1
    for m in range(3):
        loads[2 + m].wait()
        count = n_rows if m < 2 else samples
        part = jnp.dot(activated, mod[m], preferred_element_type=F32)
        packf[m * n_rows : m * n_rows + count, :] = part[0:count, :]
    pack[...] = packf[...].astype(BF16)

    pl.semaphore_wait(barrier, n_sp - 1 + n_td - 1)
    a_copies = []
    for o in range(1, n_sp):
        copy = pltpu.make_async_remote_copy(
            src_ref=pack, dst_ref=packs.at[o - 1], send_sem=a_s.at[o - 1], recv_sem=a_r.at[o - 1],
            device_id={"sp": lax.rem(sp + o, n_sp)}, device_id_type=MESH,
        )
        copy.start()
        a_copies.append(copy)

    chunk = 64

    def normalise(src, dst, first, last):
        def body(i, carry):
            rows = pl.ds(pl.multiple_of(i * chunk, chunk), chunk)
            x = src[rows, :].astype(F32)
            x = x - jnp.mean(x, axis=-1, keepdims=True)
            spread = jnp.mean(x * x, axis=-1, keepdims=True)
            x = x * lax.rsqrt(spread + NORM_EPSILON)
            for t in range(n_tp):
                dst[t, rows, :] = x[:, t * group : (t + 1) * group]
            return carry

        lax.fori_loop(first, last, body, 0)

    loads[5].wait()
    normalise(ctx, xnc, 0, n_ctx // chunk)
    loads[6].wait()
    normalise(lat, xn, 0, tok // chunk)

    for copy in a_copies:
        copy.wait_recv()
    summed = packf[...]
    for o in range(1, n_sp):
        summed = summed + packs[o - 1].astype(F32)
    total[...] = summed
    for d in range(n_dp):
        rows = [
            total[source : source + 1, :]
            for source in (d, n_rows + d, 2 * n_rows + d, samples, n_rows + samples)
        ]
        rows.append(jnp.zeros((3, cols), F32))
        sendb[d] = jnp.concatenate(rows, axis=0).astype(BF16)
    b_copies = {}
    for o in range(n_tp):
        for e in range(n_dp):
            if o == 0 and e == 0:
                continue
            d = lax.rem(dp + e, n_dp)
            copy = pltpu.make_async_remote_copy(
                src_ref=sendb.at[d], dst_ref=slots.at[o * n_dp + dp],
                send_sem=b_s.at[o * n_dp + e], recv_sem=b_r.at[o * n_dp + e],
                device_id={"tp": partner(o), "dp": d}, device_id_type=MESH,
            )
            copy.start()
            b_copies[o, e] = copy
    slots[dp] = sendb[dp]

    for load in loads[7:14]:
        load.wait()
    groups = tok // GRID_W
    for g in range(groups):
        row = pl.ds(sp * groups + g, 1)
        span = slice(g * GRID_W, (g + 1) * GRID_W)
        cosv[span, :] = rowt[0, row, :] + colt[0]
        sinv[span, :] = rowt[1, row, :] + colt[1]
    for j in range(width // LANES):
        span = slice(j * LANES, (j + 1) * LANES)
        wall[span, q_width:] = kvw[:, span].astype(F32).T.astype(BF16)

    def condition(src, dst, count, o, g, shift_row, scale_row):
        scale = 1.0 + modv[o, scale_row : scale_row + 1, :]
        shift = modv[o, shift_row : shift_row + 1, :]
        for i in range(0, count, chunk):
            rows = slice(i, i + chunk)
            dst[rows, :] = (src[g, rows, :] * scale + shift).astype(BF16)

    c_copies = []
    for o in range(n_tp):
        for e in range(n_dp):
            if o or e:
                b_copies[o, e].wait_recv()
        for d in range(n_dp):
            modv[o, :, d * cols : (d + 1) * cols] = slots[o * n_dp + d].astype(F32)
        g = owner(o)
        weight_rows = pl.ds(pl.multiple_of(g * group, group), group)
        condition(xnc, nrmc, n_ctx, o, g, 3, 4)
        u = jnp.dot(nrmc[...], wall[weight_rows, q_width:], preferred_element_type=F32)
        if o:
            u = accc[...] + u
        if o < n_tp - 1:
            accc[...] = u
        else:
            cxb[0] = u.astype(BF16)
            for r in range(1, n_sp):
                copy = pltpu.make_async_remote_copy(
                    src_ref=cxb.at[0], dst_ref=cxb.at[r], send_sem=c_s.at[r - 1],
                    recv_sem=c_r.at[r - 1], device_id={"sp": lax.rem(sp + r, n_sp)},
                    device_id_type=MESH,
                )
                copy.start()
                c_copies.append(copy)
        condition(xn, nrm, tok, o, g, 0, 1)
        u = jnp.dot(nrm[...], wall[weight_rows, :], preferred_element_type=F32)
        if o:
            u = acc[...] + u
        acc[...] = u

    half = HEAD_SIZE // 2
    quarter = half // 2

    def turn(u, cosine, sine):
        w = u.shape[1]
        lane = lax.broadcasted_iota(jnp.int32, u.shape, 1)
        first = lax.rem(lane, half) < quarter
        swapped = jnp.where(first, pltpu.roll(u, w - quarter, 1), pltpu.roll(u, quarter, 1))
        return u * cosine + swapped * sine

    def low_half(shape):
        return lax.broadcasted_iota(jnp.int32, shape, 1) < HEAD_SIZE

    def expand(x, at):
        low = low_half(x.shape)
        other = pltpu.roll(x, HEAD_SIZE, 1)
        span = slice(at, at + x.shape[0])
        kd[span, :] = jnp.where(low, x, other).astype(BF16)
        vd[span, :] = jnp.where(low, other, x).astype(BF16)

    u = acc[:, q_width:]
    kv_rows = jnp.where(low_half(u.shape), turn(u, cosv[...], sinv[...]), u)
    kvb[reach : reach + tok, :] = kv_rows.astype(BF16)

    up = pltpu.make_async_remote_copy(
        src_ref=kvb.at[pl.ds(tok, reach)], dst_ref=kvb.at[pl.ds(0, reach)],
        send_sem=h_s.at[0], recv_sem=h_r.at[0],
        device_id={"sp": lax.rem(sp + 1, n_sp)}, device_id_type=MESH,
    )
    down = pltpu.make_async_remote_copy(
        src_ref=kvb.at[pl.ds(reach, reach)], dst_ref=kvb.at[pl.ds(reach + tok, reach)],
        send_sem=h_s.at[1], recv_sem=h_r.at[1],
        device_id={"sp": lax.rem(sp + n_sp - 1, n_sp)}, device_id_type=MESH,
    )

    @pl.when(sp < n_sp - 1)
    def _():
        up.start()

    @pl.when(sp > 0)
    def _():
        down.start()

    expand(kv_rows, reach)

    factor = HEAD_SIZE ** (-0.5)
    for p in range(pairs):
        t = turn(acc[:, p * LANES : (p + 1) * LANES], cosv[...], sinv[...]) * factor
        low = low_half(t.shape)
        for parity, kept in ((0, jnp.where(low, t, 0.0)), (1, jnp.where(low, 0.0, t))):
            kept = kept.astype(BF16)
            at = (2 * p + parity) * reach
            for b in range(blocks):
                q4[b, at : at + reach, :] = kept[b * reach : (b + 1) * reach, :]

    window = tok + 2 * reach
    m_rows = heads * reach
    nt = (((1,), (1,)), ((), ()))

    def per_head(ref):
        return jnp.concatenate([jnp.full((reach, 1), ref[h], F32) for h in range(heads)], axis=0)

    n_all_ctx = n_sp * n_ctx
    delta = lax.broadcasted_iota(jnp.int32, (m_rows, reach), 1) - lax.rem(
        lax.broadcasted_iota(jnp.int32, (m_rows, reach), 0), reach
    )
    far = 4 * reach
    low_edge = jnp.where(sp == 0, far, 0)
    high_edge = jnp.where(sp == n_sp - 1, -far, 0)

    def scores(b, first, count):
        keys = kd[first : first + count, :]
        return lax.dot_general(q4[b], keys, nt, preferred_element_type=F32)

    def tiles(s):
        return [s[:, c * LANES : (c + 1) * LANES] for c in range(s.shape[1] // LANES)]

    def soften(parts, highest):
        powers = [jnp.exp(s - highest) for s in parts]
        mass = powers[0]
        for e in powers[1:]:
            mass = mass + e
        return powers, jnp.sum(mass, axis=-1, keepdims=True)

    def top_of(parts):
        top = parts[0]
        for s in parts[1:]:
            top = jnp.maximum(top, s)
        return jnp.max(top, axis=-1, keepdims=True)

    def weigh(powers, first):
        e = jnp.concatenate(powers, axis=1).astype(BF16)
        return jnp.dot(e, vd[first : first + e.shape[1], :], preferred_element_type=F32)

    def within(b):
        first, last = max(b - 1, 0), min(b + 1, blocks - 1)
        at = reach + first * reach
        parts = tiles(scores(b, at, (last - first + 1) * reach))
        if b > 0:
            parts[0] = jnp.where(delta >= 0, parts[0], MASKED)
        if b < blocks - 1:
            parts[-1] = jnp.where(delta <= 0, parts[-1], MASKED)
        sunk = per_head(sink)
        highest = jnp.maximum(top_of(parts), sunk)
        powers, mass = soften(parts, highest)
        return highest, mass + jnp.exp(sunk - highest), weigh(powers, at)

    g_copies = {}

    def beyond(b, state):
        highest, mass, weighed = state
        column = per_head(bias)
        groups = [(window, [s + column for s in tiles(scores(b, window, n_all_ctx))])]
        if b == 0:
            s = scores(b, 0, reach)
            groups.append((0, [jnp.where(delta >= low_edge, s, MASKED)]))
        if b == blocks - 1:
            s = scores(b, reach + tok, reach)
            groups.append((reach + tok, [jnp.where(delta <= high_edge, s, MASKED)]))
        top = jnp.maximum(top_of(sum([parts for _, parts in groups], [])), highest)
        fade = jnp.exp(highest - top)
        mass = mass * fade
        weighed = weighed * fade
        for at, parts in groups:
            powers, more = soften(parts, top)
            mass = mass + more
            weighed = weighed + weigh(powers, at)
        result = weighed / mass
        low = low_half((reach, LANES))
        for p in range(pairs):
            even = result[2 * p * reach : (2 * p + 1) * reach, :]
            odd = result[(2 * p + 1) * reach : (2 * p + 2) * reach, :]
            att[0, b, :, p * LANES : (p + 1) * LANES] = jnp.where(low, even, odd).astype(BF16)
        for o in direct:
            copy = pltpu.make_async_remote_copy(
                src_ref=att.at[0, b], dst_ref=att.at[o, b], send_sem=g_s.at[b, o - 1],
                recv_sem=g_r.at[b, o - 1], device_id={"tp": partner(o)}, device_id_type=MESH,
            )
            copy.start()
            g_copies[b, o] = copy

    def forward(b):
        for o in direct:
            g_copies[b, o].wait_recv()
            part = pl.ds((o - 1) * (reach // 2), reach // 2)
            copy = pltpu.make_async_remote_copy(
                src_ref=att.at[o, b, part], dst_ref=att.at[3, b, part],
                send_sem=g_s.at[b, 1 + o], recv_sem=g_r.at[b, 1 + o],
                device_id={"tp": partner(3 - o)}, device_id_type=MESH,
            )
            copy.start()
            g_copies[b, 2 + o] = copy

    order = list(range(1, blocks - 1)) + ([0, blocks - 1] if blocks > 1 else [0])
    states = {}
    for b in order:
        states[b] = within(b)
    for r in range(1, n_sp):
        c_copies[r - 1].wait_recv()
    for r in range(n_sp):
        expand(cxb[r].astype(F32), window + r * n_ctx)
    for b in order:
        if b == 0:
            @pl.when(sp > 0)
            def _():
                up.wait_recv()

            @pl.when(sp == 0)
            def _():
                kvb[0:reach, :] = jnp.zeros((reach, LANES), BF16)

            expand(kvb[0:reach, :].astype(F32), 0)
        if b == blocks - 1:
            @pl.when(sp < n_sp - 1)
            def _():
                down.wait_recv()

            @pl.when(sp == n_sp - 1)
            def _():
                kvb[reach + tok : window, :] = jnp.zeros((reach, LANES), BF16)

            expand(kvb[reach + tok : window, :].astype(F32), reach + tok)
        beyond(b, states[b])

    loads[14].wait()
    out_cols = ow.shape[1]
    mine = pl.ds(pl.multiple_of(tp * out_cols, out_cols), out_cols)
    gate = modv[0, 2:3, :]

    def project(b, o):
        w = ow[pl.ds(pl.multiple_of(owner(o) * q_width, q_width), q_width), :]
        return jnp.dot(att[o, b], w, preferred_element_type=F32)

    for b in order:
        if relayed:
            forward(b)
        mixed = project(b, 0)
        for o in direct:
            if not relayed:
                g_copies[b, o].wait_recv()
            mixed = mixed + project(b, o)
        outv[b * reach : (b + 1) * reach, :] = mixed
    for b in order:
        rows = slice(b * reach, (b + 1) * reach)
        mixed = outv[rows, :]
        if relayed:
            g_copies[b, 3].wait_recv()
            g_copies[b, 4].wait_recv()
            mixed = mixed + project(b, 3)
        outv[rows, :] = lat[rows, mine].astype(F32) + gate * mixed

    for copy in a_copies + list(b_copies.values()) + c_copies + list(g_copies.values()):
        copy.wait_send()

    @pl.when(sp < n_sp - 1)
    def _():
        up.wait_send()

    @pl.when(sp > 0)
    def _():
        down.wait_send()


def per_device(
    latent, conditioning, context_cond, modulation, context, query_weight, key_projection,
    value_projection, out_weight, sink_head_logit, prefix_logit_bias,
):
    n_sp, n_tp, n_dp = lax.axis_size("sp"), lax.axis_size("tp"), lax.axis_size("dp")
    samples = conditioning.shape[0]
    _, tok, width = latent.shape
    n_ctx = context.shape[1]
    depth, cols = modulation.shape[1:]
    q_width = query_weight.shape[1]
    heads = q_width // HEAD_SIZE
    out_cols = out_weight.shape[1]
    blocks = tok // WINDOW_REACH
    window = tok + 2 * WINDOW_REACH
    keys = window + n_sp * n_ctx
    n_td = n_tp * n_dp
    act_rows = -(-(samples + 1) // 8) * 8
    pack_rows = -(-(3 * samples + 2) // 8) * 8
    row_table, col_table = rotary_tables(n_sp * tok // GRID_W)
    vm = pltpu.VMEM
    dma = pltpu.SemaphoreType.DMA
    group = n_dp * cols
    scratch = [
        vm((tok, width), BF16), vm((samples, depth), BF16), vm((depth,), BF16),
        vm((3, depth, cols), BF16), vm((n_ctx, width), BF16), vm((width, q_width + LANES), BF16),
        vm(out_weight.shape, BF16), pltpu.SMEM((heads,), F32), pltpu.SMEM((heads,), F32),
        vm(row_table.shape, F32), vm(col_table.shape, F32),
        vm((act_rows, depth), F32), vm((pack_rows, cols), F32), vm((pack_rows, cols), BF16),
        vm((n_sp - 1, pack_rows, cols), BF16), vm((pack_rows, cols), F32),
        vm((n_dp, 8, cols), BF16), vm((n_td, 8, cols), BF16), vm((n_tp, 8, group), F32),
        vm((n_tp, tok, group), F32), vm((n_tp, n_ctx, group), F32), vm((tok, group), BF16),
        vm((n_ctx, group), BF16), vm((LANES, width), BF16), vm((tok, LANES), F32),
        vm((tok, LANES), F32), vm((tok, q_width + LANES), F32), vm((n_ctx, LANES), F32),
        vm((window, LANES), BF16), vm((n_sp, n_ctx, LANES), BF16),
        vm((keys, LANES), BF16), vm((keys, LANES), BF16),
        vm((blocks, heads * WINDOW_REACH, LANES), BF16),
        vm((n_tp, blocks, WINDOW_REACH, q_width), BF16),
        dma((15,)), dma((n_sp - 1,)), dma((n_sp - 1,)), dma((n_td,)),
        dma((n_td,)), dma((2,)), dma((2,)), dma((n_sp - 1,)), dma((n_sp - 1,)),
        dma((blocks, n_tp)), dma((blocks, n_tp)),
    ]
    stays = pl.BlockSpec(memory_space=pltpu.HBM)
    out = pl.pallas_call(
        functools.partial(block_kernel, (n_sp, n_tp, n_dp, samples)),
        out_shape=pltpu.VMEM((tok, out_cols), F32),
        in_specs=[stays] * 13,
        out_specs=pl.BlockSpec(memory_space=pltpu.VMEM),
        scratch_shapes=scratch,
        compiler_params=pltpu.CompilerParams(
            collective_id=0, has_side_effects=True, vmem_limit_bytes=66000000
        ),
        name="fused_block",
    )(
        latent[0], conditioning, context_cond, modulation, context[0], query_weight,
        key_projection.T, value_projection.T, out_weight, sink_head_logit, prefix_logit_bias,
        jnp.asarray(row_table), jnp.asarray(col_table),
    )
    return out[None]


def solution(mesh):
    placed = (
        P("dp", "sp", None),
        P(None, "sp"),
        P("sp"),
        P(None, "sp", ("tp", "dp")),
        P("dp", "sp", None),
        P(None, "tp"),
        P(None, "tp"),
        P(None, "tp"),
        P(None, "tp"),
        P("tp"),
        P("tp"),
    )
    return jax.shard_map(
        per_device, mesh=mesh, in_specs=placed, out_specs=P("dp", "sp", "tp"), check_vma=False
    )
```

time: 29.3 us -> 29.6 us (1.010)
  Pallas kernels: 28.3 us -> 28.6 us
    pallas_call x1, Pallas kernels: 28.3 us -> 28.6 us  [per_device(): pl.pallas_call(functools.partial(block_kernel, (n_sp, n_tp, n_dp, samples...]
where the time goes in v2:
time: 29.6 us; the launch traced here: 29.5 us
  Pallas kernels  28.6 us (97%)
  local copies, waits for them, and re-layouts  0.88 us (3%)
    pallas_call x1, Pallas kernels, per_device(): pl.pallas_call(functools.partial(block_kernel, (n_sp, n_tp, n_dp, samples...  28.6 us
    unnamed x1, local copies, waits for them, and re-layouts  0.88 us

profile of v2, /device:TPU:0, one launch (start us, length us, event | category | flops | bytes accessed | tf_op | source)
XLA Modules:
  0.0 29.5 jit_solution(15692352723913415341)
XLA Ops:
  0.0 28.6 %fused_block.1 = f32[384,512]{1,0:T(8,128)S(1)} custom-call(bf16[384,2048]{1,0:T(8,128)(2,1)} %bitcast.6, bf16[2,512]{1,0:T(2,128)(2,1)} %cond_hbm.1, bf16[512]{0:T(512)(128)(2,1)} %cctx_hbm.1, bf16[3,512,256]{2,1,0:T(8,128)(2,1)} %mod_hbm.1, bf16[64,2048]{1,0:T(8,128)(2,1)} %bitcast.7, bf16[2048,256]{1,0:T(8,128)(2,1)} %qw_hbm.1, bf16[64,2048]{1,0:T(8,128)(2,1)} %bitcast.8, ...), custom_call_target="tpu_custom_call" | custom-call | tf_op jit(solution)/shard_map/fused_block/pallas_call | solution.py:495
  28.6 0.9 %copy.15 = f32[1,384,512]{2,1,0:T(8,128)} copy(f32[1,384,512]{2,1,0:T(8,128)S(1)} %bitcast.5) | data formatting | bytes 1572864

commit v3 on v2

--- a/solution.py
+++ b/solution.py
@@ -283,15 +283,10 @@
                 q4[b, at : at + reach, :] = kept[b * reach : (b + 1) * reach, :]
 
     window = tok + 2 * reach
-    m_rows = heads * reach
     nt = (((1,), (1,)), ((), ()))
-
-    def per_head(ref):
-        return jnp.concatenate([jnp.full((reach, 1), ref[h], F32) for h in range(heads)], axis=0)
-
     n_all_ctx = n_sp * n_ctx
-    delta = lax.broadcasted_iota(jnp.int32, (m_rows, reach), 1) - lax.rem(
-        lax.broadcasted_iota(jnp.int32, (m_rows, reach), 0), reach
+    delta = lax.broadcasted_iota(jnp.int32, (reach, reach), 1) - lax.broadcasted_iota(
+        jnp.int32, (reach, reach), 0
     )
     far = 4 * reach
     low_edge = jnp.where(sp == 0, far, 0)
@@ -301,14 +296,16 @@
         keys = kd[first : first + count, :]
         return lax.dot_general(q4[b], keys, nt, preferred_element_type=F32)
 
-    def tiles(s):
-        return [s[:, c * LANES : (c + 1) * LANES] for c in range(s.shape[1] // LANES)]
+    def tiles(s, h):
+        rows = slice(h * reach, (h + 1) * reach)
+        return [s[rows, c * LANES : (c + 1) * LANES] for c in range(s.shape[1] // LANES)]
 
     def soften(parts, highest):
         powers = [jnp.exp(s - highest) for s in parts]
         mass = powers[0]
         for e in powers[1:]:
             mass = mass + e
+        powers = jnp.concatenate([e.astype(BF16) for e in powers], axis=1)
         return powers, jnp.sum(mass, axis=-1, keepdims=True)
 
     def top_of(parts):
@@ -318,48 +315,62 @@
         return jnp.max(top, axis=-1, keepdims=True)
 
     def weigh(powers, first):
-        e = jnp.concatenate(powers, axis=1).astype(BF16)
+        e = jnp.concatenate(powers, axis=0)
         return jnp.dot(e, vd[first : first + e.shape[1], :], preferred_element_type=F32)
 
     def within(b):
         first, last = max(b - 1, 0), min(b + 1, blocks - 1)
         at = reach + first * reach
-        parts = tiles(scores(b, at, (last - first + 1) * reach))
-        if b > 0:
-            parts[0] = jnp.where(delta >= 0, parts[0], MASKED)
-        if b < blocks - 1:
-            parts[-1] = jnp.where(delta <= 0, parts[-1], MASKED)
-        sunk = per_head(sink)
-        highest = jnp.maximum(top_of(parts), sunk)
-        powers, mass = soften(parts, highest)
-        return highest, mass + jnp.exp(sunk - highest), weigh(powers, at)
+        s = scores(b, at, (last - first + 1) * reach)
+        tops, masses, powers = [], [], []
+        for h in range(heads):
+            parts = tiles(s, h)
+            if b > 0:
+                parts[0] = jnp.where(delta >= 0, parts[0], MASKED)
+            if b < blocks - 1:
+                parts[-1] = jnp.where(delta <= 0, parts[-1], MASKED)
+            highest = jnp.maximum(top_of(parts), sink[h])
+            e, mass = soften(parts, highest)
+            tops.append(highest)
+            masses.append(mass + jnp.exp(sink[h] - highest))
+            powers.append(e)
+        return tops, masses, weigh(powers, at)
 
     g_copies = {}
 
     def beyond(b, state):
-        highest, mass, weighed = state
-        column = per_head(bias)
-        groups = [(window, [s + column for s in tiles(scores(b, window, n_all_ctx))])]
+        tops, masses, weighed = state
+        parts_of = [(window, scores(b, window, n_all_ctx))]
         if b == 0:
-            s = scores(b, 0, reach)
-            groups.append((0, [jnp.where(delta >= low_edge, s, MASKED)]))
+            parts_of.append((0, scores(b, 0, reach)))
         if b == blocks - 1:
-            s = scores(b, reach + tok, reach)
-            groups.append((reach + tok, [jnp.where(delta <= high_edge, s, MASKED)]))
-        top = jnp.maximum(top_of(sum([parts for _, parts in groups], [])), highest)
-        fade = jnp.exp(highest - top)
-        mass = mass * fade
-        weighed = weighed * fade
-        for at, parts in groups:
-            powers, more = soften(parts, top)
-            mass = mass + more
-            weighed = weighed + weigh(powers, at)
-        result = weighed / mass
+            parts_of.append((reach + tok, scores(b, reach + tok, reach)))
+        fades, powers = [], [[] for _ in parts_of]
+        for h in range(heads):
+            groups = [[s + bias[h] for s in tiles(parts_of[0][1], h)]]
+            if b == 0:
+                groups.append([jnp.where(delta >= low_edge, parts_of[-1][1][h * reach : (h + 1) * reach], MASKED)])
+            if b == blocks - 1:
+                groups.append([jnp.where(delta <= high_edge, parts_of[-1][1][h * reach : (h + 1) * reach], MASKED)])
+            top = jnp.maximum(top_of(sum(groups, [])), tops[h])
+            fade = jnp.exp(tops[h] - top)
+            mass = masses[h] * fade
+            for i, parts in enumerate(groups):
+                e, more = soften(parts, top)
+                powers[i].append(e)
+                mass = mass + more
+            share = 1.0 / mass
+            fades.append((fade * share, share))
+        more = weigh(powers[0], window)
+        for i in range(1, len(parts_of)):
+            more = more + weigh(powers[i], parts_of[i][0])
         low = low_half((reach, LANES))
         for p in range(pairs):
-            even = result[2 * p * reach : (2 * p + 1) * reach, :]
-            odd = result[(2 * p + 1) * reach : (2 * p + 2) * reach, :]
-            att[0, b, :, p * LANES : (p + 1) * LANES] = jnp.where(low, even, odd).astype(BF16)
+            halves = []
+            for h in (2 * p, 2 * p + 1):
+                rows = slice(h * reach, (h + 1) * reach)
+                halves.append(weighed[rows, :] * fades[h][0] + more[rows, :] * fades[h][1])
+            att[0, b, :, p * LANES : (p + 1) * LANES] = jnp.where(low, *halves).astype(BF16)
         for o in direct:
             copy = pltpu.make_async_remote_copy(
                 src_ref=att.at[0, b], dst_ref=att.at[o, b], send_sem=g_s.at[b, o - 1],

time: 29.6 us -> 28.3 us (0.956)
  Pallas kernels: 28.6 us -> 27.3 us
    pallas_call x1, Pallas kernels: 28.6 us -> 27.3 us  [per_device(): pl.pallas_call(functools.partial(block_kernel, (n_sp, n_tp, n_dp, samples...]
where the time goes in v3:
time: 28.3 us; the launch traced here: 28.2 us
  Pallas kernels  27.3 us (96%)
  local copies, waits for them, and re-layouts  0.88 us (3%)
    pallas_call x1, Pallas kernels, per_device(): pl.pallas_call(functools.partial(block_kernel, (n_sp, n_tp, n_dp, samples...  27.3 us
    unnamed x1, local copies, waits for them, and re-layouts  0.88 us

profile of v3, /device:TPU:0, one launch (start us, length us, event | category | flops | bytes accessed | tf_op | source)
XLA Modules:
  0.0 28.2 jit_solution(14357751885662827790)
XLA Ops:
  0.0 27.3 %fused_block.1 = f32[384,512]{1,0:T(8,128)S(1)} custom-call(bf16[384,2048]{1,0:T(8,128)(2,1)} %bitcast.6, bf16[2,512]{1,0:T(2,128)(2,1)} %cond_hbm.1, bf16[512]{0:T(512)(128)(2,1)} %cctx_hbm.1, bf16[3,512,256]{2,1,0:T(8,128)(2,1)} %mod_hbm.1, bf16[64,2048]{1,0:T(8,128)(2,1)} %bitcast.7, bf16[2048,256]{1,0:T(8,128)(2,1)} %qw_hbm.1, bf16[64,2048]{1,0:T(8,128)(2,1)} %bitcast.8, ...), custom_call_target="tpu_custom_call" | custom-call | tf_op jit(solution)/shard_map/fused_block/pallas_call | solution.py:506
  27.3 0.9 %copy.15 = f32[1,384,512]{2,1,0:T(8,128)} copy(f32[1,384,512]{2,1,0:T(8,128)S(1)} %bitcast.5) | data formatting | bytes 1572864

commit v4 on v3

--- a/solution.py
+++ b/solution.py
@@ -41,12 +41,12 @@
 def block_kernel(
     dims,
     lat_hbm, cond_hbm, cctx_hbm, mod_hbm, ctx_hbm, qw_hbm, kw_hbm, vw_hbm, ow_hbm,
-    sink_hbm, bias_hbm, rowt_hbm, colt_hbm,
+    sink_hbm, bias_hbm, turn_hbm,
     outv,
-    lat, cond, cctx, mod, ctx, wall, ow, sink, bias, rowt, colt,
+    lat, cond, cctx, mod, ctx, wall, ow, sink, bias, angles,
     act, packf, pack, packs, total, sendb, slots, modv,
-    xn, xnc, nrm, nrmc, kvw, cosv, sinv, acc, accc, kvb, cxb, kd, vd, q4, att,
-    in_sem, a_s, a_r, b_s, b_r, h_s, h_r, c_s, c_r, g_s, g_r,
+    xn, xnc, nrm, nrmc, kvw, cosv, sinv, acc, accc, kvb, cxs, cxb, kd, vd, q4, att,
+    in_sem, a_s, a_r, x_s, x_r, b_s, b_r, h_s, h_r, c_s, c_r, g_s, g_r,
 ):
     n_sp, n_tp, n_dp, samples = dims
     sp, tp, dp = lax.axis_index("sp"), lax.axis_index("tp"), lax.axis_index("dp")
@@ -55,7 +55,9 @@
     tok, width = lat.shape
     cols = mod.shape[2]
     group = n_dp * cols
-    n_ctx = ctx.shape[0]
+    n_ctx = ctx.shape[1]
+    core, lead, pair = lax.rem(dp, 2), dp - lax.rem(dp, 2) + 1, dp // 2
+    n_pairs = n_dp // 2
     reach = WINDOW_REACH
     blocks = tok // reach
     q_width = wall.shape[1] - LANES
@@ -64,9 +66,11 @@
 
     barrier = pltpu.get_barrier_semaphore()
     for o in range(1, n_sp):
-        pl.semaphore_signal(
-            barrier, inc=1, device_id={"sp": lax.rem(sp + o, n_sp)}, device_id_type=MESH
-        )
+        for d in (dp, 2 * pair + 1 - core):
+            pl.semaphore_signal(
+                barrier, inc=1, device_id={"sp": lax.rem(sp + o, n_sp), "dp": d},
+                device_id_type=MESH,
+            )
     for o in range(1, n_td):
         lin = lax.rem(me + o, n_td)
         pl.semaphore_signal(
@@ -89,22 +93,29 @@
         return partner(o) if relayed else lax.rem(tp + n_tp - o, n_tp)
 
     pairs_in = [
-        (cond_hbm, cond), (cctx_hbm, cctx), (mod_hbm.at[0], mod.at[0]), (mod_hbm.at[1], mod.at[1]),
-        (mod_hbm.at[2], mod.at[2]), (ctx_hbm, ctx), (lat_hbm, lat),
-        (kw_hbm, kvw.at[pl.ds(0, HEAD_SIZE)]), (vw_hbm, kvw.at[pl.ds(HEAD_SIZE, HEAD_SIZE)]),
-        (rowt_hbm, rowt), (colt_hbm, colt), (qw_hbm, wall.at[:, pl.ds(0, q_width)]),
-        (sink_hbm, sink), (bias_hbm, bias), (ow_hbm, ow),
+        (cond_hbm, cond, 0), (cctx_hbm, cctx, 1), (mod_hbm, mod, 2), (ctx_hbm, ctx.at[0], 3),
+        (lat_hbm, lat, 4), (kw_hbm, kvw.at[pl.ds(0, HEAD_SIZE)], 5),
+        (vw_hbm, kvw.at[pl.ds(HEAD_SIZE, HEAD_SIZE)], 5), (turn_hbm, angles, 6),
+        (qw_hbm, wall.at[:, pl.ds(0, q_width)], 7), (sink_hbm, sink, 8), (bias_hbm, bias, 9),
+        (ow_hbm, ow, 10),
     ]
-    loads = [
-        pltpu.make_async_copy(src, dst, in_sem.at[i]) for i, (src, dst) in enumerate(pairs_in)
-    ]
-    for load in loads[:6]:
+    loads = [pltpu.make_async_copy(src, dst, in_sem.at[i]) for src, dst, i in pairs_in]
+    for load in loads[:4]:
         load.start()
+
+    def remote(src, dst, left, arrived, **device):
+        return pltpu.make_async_remote_copy(
+            src_ref=src, dst_ref=dst, send_sem=left, recv_sem=arrived, device_id=device,
+            device_id_type=MESH,
+        )
+
+    def bytes_of(ref, semaphore):
+        pltpu.make_async_copy(ref, ref, semaphore).wait()
 
     act[...] = jnp.zeros_like(act)
     loads[0].wait()
     loads[1].wait()
-    for load in loads[6:]:
+    for load in loads[4:]:
         load.start()
     act[0:samples, :] = cond[...].astype(F32)
     act[samples : samples + 1, :] = cctx[...].astype(F32).reshape(1, cctx.shape[0])
@@ -112,22 +123,30 @@
     activated = (v / (1.0 + jnp.exp(-v))).astype(BF16)
     packf[...] = jnp.zeros_like(packf)
     n_rows = samples + 1
+    loads[2].wait()
     for m in range(3):
-        loads[2 + m].wait()
         count = n_rows if m < 2 else samples
         part = jnp.dot(activated, mod[m], preferred_element_type=F32)
         packf[m * n_rows : m * n_rows + count, :] = part[0:count, :]
     pack[...] = packf[...].astype(BF16)
 
-    pl.semaphore_wait(barrier, n_sp - 1 + n_td - 1)
-    a_copies = []
-    for o in range(1, n_sp):
-        copy = pltpu.make_async_remote_copy(
-            src_ref=pack, dst_ref=packs.at[o - 1], send_sem=a_s.at[o - 1], recv_sem=a_r.at[o - 1],
-            device_id={"sp": lax.rem(sp + o, n_sp)}, device_id_type=MESH,
+    pl.semaphore_wait(barrier, 2 * (n_sp - 1) + n_td - 1)
+    a_copies = [
+        remote(
+            pack, packs.at[2 * o - 1 + core if o else 0], a_s.at[0], a_r.at[0],
+            sp=lax.rem(sp + o, n_sp), dp=lead,
         )
+        for o in range(n_sp)
+    ]
+    for copy in a_copies[1:]:
         copy.start()
-        a_copies.append(copy)
+    spare = remote(ctx.at[0], ctx.at[1], x_s.at[0], x_r.at[0], dp=lead)
+    loads[3].wait()
+
+    @pl.when(core == 0)
+    def _():
+        a_copies[0].start()
+        spare.start()
 
     chunk = 64
 
@@ -144,47 +163,65 @@
 
         lax.fori_loop(first, last, body, 0)
 
-    loads[5].wait()
-    normalise(ctx, xnc, 0, n_ctx // chunk)
-    loads[6].wait()
+    def normalise_context(which):
+        for i in range(0, n_ctx, chunk):
+            x = ctx[which, i : i + chunk, :].astype(F32)
+            x = x - jnp.mean(x, axis=-1, keepdims=True)
+            spread = jnp.mean(x * x, axis=-1, keepdims=True)
+            x = x * lax.rsqrt(spread + NORM_EPSILON)
+            at = which * n_ctx + i
+            for t in range(n_tp):
+                xnc[t, at : at + chunk, :] = x[:, t * group : (t + 1) * group]
+
+    loads[4].wait()
     normalise(lat, xn, 0, tok // chunk)
 
-    for copy in a_copies:
-        copy.wait_recv()
-    summed = packf[...]
-    for o in range(1, n_sp):
-        summed = summed + packs[o - 1].astype(F32)
-    total[...] = summed
-    for d in range(n_dp):
-        rows = [
-            total[source : source + 1, :]
-            for source in (d, n_rows + d, 2 * n_rows + d, samples, n_rows + samples)
-        ]
-        rows.append(jnp.zeros((3, cols), F32))
-        sendb[d] = jnp.concatenate(rows, axis=0).astype(BF16)
-    b_copies = {}
-    for o in range(n_tp):
-        for e in range(n_dp):
-            if o == 0 and e == 0:
-                continue
-            d = lax.rem(dp + e, n_dp)
-            copy = pltpu.make_async_remote_copy(
-                src_ref=sendb.at[d], dst_ref=slots.at[o * n_dp + dp],
-                send_sem=b_s.at[o * n_dp + e], recv_sem=b_r.at[o * n_dp + e],
-                device_id={"tp": partner(o), "dp": d}, device_id_type=MESH,
-            )
+    @pl.when(core == 1)
+    def _():
+        normalise_context(0)
+        spare.wait_recv()
+        normalise_context(1)
+
+
+    b_copies = [
+        remote(
+            sendb.at[lax.rem(dp + e, n_dp)], slots.at[o, pair], b_s.at[o], b_r.at[o],
+            tp=partner(o), dp=lax.rem(dp + e, n_dp),
+        )
+        for o in range(n_tp)
+        for e in range(n_dp)
+        if o or e
+    ]
+
+    @pl.when(core == 1)
+    def _():
+        bytes_of(packs, a_r.at[0])
+        for c in range(2):
+            summed = packf[...] if c else packs[0].astype(F32)
+            for o in range(1, n_sp):
+                summed = summed + packs[2 * o - 1 + c].astype(F32)
+            total[c] = summed
+        for d in range(n_dp):
+            for c in range(2):
+                rows = [
+                    total[c, source : source + 1, :]
+                    for source in (d, n_rows + d, 2 * n_rows + d, samples, n_rows + samples)
+                ]
+                rows.append(jnp.zeros((3, cols), F32))
+                sendb[d, c] = jnp.concatenate(rows, axis=0).astype(BF16)
+        for copy in b_copies:
             copy.start()
-            b_copies[o, e] = copy
-    slots[dp] = sendb[dp]
-
-    for load in loads[7:14]:
+        slots[0, pair] = sendb[dp]
+
+    bytes_of(kvw, in_sem.at[5])
+    for load in loads[7:11]:
         load.wait()
     groups = tok // GRID_W
     for g in range(groups):
-        row = pl.ds(sp * groups + g, 1)
+        row = pl.ds(GRID_W + sp * groups + g, 1)
         span = slice(g * GRID_W, (g + 1) * GRID_W)
-        cosv[span, :] = rowt[0, row, :] + colt[0]
-        sinv[span, :] = rowt[1, row, :] + colt[1]
+        cosv[span, :] = angles[0, row, :] + angles[0, 0:GRID_W, :]
+        sinv[span, :] = angles[1, row, :] + angles[1, 0:GRID_W, :]
     for j in range(width // LANES):
         span = slice(j * LANES, (j + 1) * LANES)
         wall[span, q_width:] = kvw[:, span].astype(F32).T.astype(BF16)
@@ -196,31 +233,47 @@
             rows = slice(i, i + chunk)
             dst[rows, :] = (src[g, rows, :] * scale + shift).astype(BF16)
 
-    c_copies = []
+    c_copies = [remote(cxs.at[0], cxb.at[0], c_s.at[0], c_r.at[0], dp=dp - core)]
+    for r in range(1, n_sp):
+        for c in range(2):
+            c_copies.append(
+                remote(
+                    cxs.at[c], cxb.at[r], c_s.at[c], c_r.at[0],
+                    sp=lax.rem(sp + r, n_sp), dp=2 * pair + c,
+                )
+            )
     for o in range(n_tp):
-        for e in range(n_dp):
-            if o or e:
-                b_copies[o, e].wait_recv()
+        if o:
+            bytes_of(slots.at[o], b_r.at[o])
+        else:
+            @pl.when(core == 0)
+            def _():
+                bytes_of(slots.at[0], b_r.at[0])
+
+            if n_pairs > 1:
+                @pl.when(core == 1)
+                def _():
+                    bytes_of(slots.at[0, pl.ds(1, n_pairs - 1)], b_r.at[0])
         for d in range(n_dp):
-            modv[o, :, d * cols : (d + 1) * cols] = slots[o * n_dp + d].astype(F32)
+            modv[o, :, d * cols : (d + 1) * cols] = slots[o, d // 2, d % 2].astype(F32)
         g = owner(o)
         weight_rows = pl.ds(pl.multiple_of(g * group, group), group)
-        condition(xnc, nrmc, n_ctx, o, g, 3, 4)
-        u = jnp.dot(nrmc[...], wall[weight_rows, q_width:], preferred_element_type=F32)
-        if o:
-            u = accc[...] + u
-        if o < n_tp - 1:
-            accc[...] = u
-        else:
-            cxb[0] = u.astype(BF16)
-            for r in range(1, n_sp):
-                copy = pltpu.make_async_remote_copy(
-                    src_ref=cxb.at[0], dst_ref=cxb.at[r], send_sem=c_s.at[r - 1],
-                    recv_sem=c_r.at[r - 1], device_id={"sp": lax.rem(sp + r, n_sp)},
-                    device_id_type=MESH,
-                )
-                copy.start()
-                c_copies.append(copy)
+
+        @pl.when(core == 1)
+        def _():
+            condition(xnc, nrmc, 2 * n_ctx, o, g, 3, 4)
+            u = jnp.dot(nrmc[...], wall[weight_rows, q_width:], preferred_element_type=F32)
+            if o:
+                u = accc[...] + u
+            if o < n_tp - 1:
+                accc[...] = u
+            else:
+                cxs[0] = u[n_ctx:, :].astype(BF16)
+                cxs[1] = u[0:n_ctx, :].astype(BF16)
+                for copy in c_copies[1:] + c_copies[:1]:
+                    copy.start()
+                cxb[0] = u[0:n_ctx, :].astype(BF16)
+
         condition(xn, nrm, tok, o, g, 0, 1)
         u = jnp.dot(nrm[...], wall[weight_rows, :], preferred_element_type=F32)
         if o:
@@ -251,15 +304,13 @@
     kv_rows = jnp.where(low_half(u.shape), turn(u, cosv[...], sinv[...]), u)
     kvb[reach : reach + tok, :] = kv_rows.astype(BF16)
 
-    up = pltpu.make_async_remote_copy(
-        src_ref=kvb.at[pl.ds(tok, reach)], dst_ref=kvb.at[pl.ds(0, reach)],
-        send_sem=h_s.at[0], recv_sem=h_r.at[0],
-        device_id={"sp": lax.rem(sp + 1, n_sp)}, device_id_type=MESH,
+    up = remote(
+        kvb.at[pl.ds(tok, reach)], kvb.at[pl.ds(0, reach)], h_s.at[0], h_r.at[0],
+         sp=lax.rem(sp + 1, n_sp)
     )
-    down = pltpu.make_async_remote_copy(
-        src_ref=kvb.at[pl.ds(reach, reach)], dst_ref=kvb.at[pl.ds(reach + tok, reach)],
-        send_sem=h_s.at[1], recv_sem=h_r.at[1],
-        device_id={"sp": lax.rem(sp + n_sp - 1, n_sp)}, device_id_type=MESH,
+    down = remote(
+        kvb.at[pl.ds(reach, reach)], kvb.at[pl.ds(reach + tok, reach)], h_s.at[1], h_r.at[1],
+        sp=lax.rem(sp + n_sp - 1, n_sp),
     )
 
     @pl.when(sp < n_sp - 1)
@@ -372,31 +423,33 @@
                 halves.append(weighed[rows, :] * fades[h][0] + more[rows, :] * fades[h][1])
             att[0, b, :, p * LANES : (p + 1) * LANES] = jnp.where(low, *halves).astype(BF16)
         for o in direct:
-            copy = pltpu.make_async_remote_copy(
-                src_ref=att.at[0, b], dst_ref=att.at[o, b], send_sem=g_s.at[b, o - 1],
-                recv_sem=g_r.at[b, o - 1], device_id={"tp": partner(o)}, device_id_type=MESH,
+            g_copies[b, o] = remote(
+                att.at[0, b], att.at[o, b], g_s.at[0], g_r.at[b, 0], tp=partner(o)
             )
-            copy.start()
-            g_copies[b, o] = copy
+            g_copies[b, o].start()
 
     def forward(b):
         for o in direct:
-            g_copies[b, o].wait_recv()
             part = pl.ds((o - 1) * (reach // 2), reach // 2)
-            copy = pltpu.make_async_remote_copy(
-                src_ref=att.at[o, b, part], dst_ref=att.at[3, b, part],
-                send_sem=g_s.at[b, 1 + o], recv_sem=g_r.at[b, 1 + o],
-                device_id={"tp": partner(3 - o)}, device_id_type=MESH,
+            g_copies[b, 2 + o] = remote(
+                att.at[o, b, part], att.at[3, b, part], g_s.at[1], g_r.at[b, 1],
+                tp=partner(3 - o),
             )
-            copy.start()
-            g_copies[b, 2 + o] = copy
+            g_copies[b, 2 + o].start()
 
     order = list(range(1, blocks - 1)) + ([0, blocks - 1] if blocks > 1 else [0])
     states = {}
     for b in order:
         states[b] = within(b)
-    for r in range(1, n_sp):
-        c_copies[r - 1].wait_recv()
+
+    @pl.when(core == 0)
+    def _():
+        bytes_of(cxb, c_r.at[0])
+
+    @pl.when(core == 1)
+    def _():
+        bytes_of(cxb.at[pl.ds(1, n_sp - 1)], c_r.at[0])
+
     for r in range(n_sp):
         expand(cxb[r].astype(F32), window + r * n_ctx)
     for b in order:
@@ -422,7 +475,7 @@
             expand(kvb[reach + tok : window, :].astype(F32), reach + tok)
         beyond(b, states[b])
 
-    loads[14].wait()
+    loads[11].wait()
     out_cols = ow.shape[1]
     mine = pl.ds(pl.multiple_of(tp * out_cols, out_cols), out_cols)
     gate = modv[0, 2:3, :]
@@ -432,25 +485,38 @@
         return jnp.dot(att[o, b], w, preferred_element_type=F32)
 
     for b in order:
+        bytes_of(att.at[pl.ds(1, len(direct)), b], g_r.at[b, 0])
         if relayed:
             forward(b)
         mixed = project(b, 0)
         for o in direct:
-            if not relayed:
-                g_copies[b, o].wait_recv()
             mixed = mixed + project(b, o)
         outv[b * reach : (b + 1) * reach, :] = mixed
     for b in order:
         rows = slice(b * reach, (b + 1) * reach)
         mixed = outv[rows, :]
         if relayed:
-            g_copies[b, 3].wait_recv()
-            g_copies[b, 4].wait_recv()
+            bytes_of(att.at[3, b], g_r.at[b, 1])
             mixed = mixed + project(b, 3)
         outv[rows, :] = lat[rows, mine].astype(F32) + gate * mixed
 
-    for copy in a_copies + list(b_copies.values()) + c_copies + list(g_copies.values()):
-        copy.wait_send()
+    bytes_of(att.at[pl.ds(1, len(direct))], g_s.at[0])
+    if relayed:
+        bytes_of(att.at[3], g_s.at[1])
+
+    @pl.when(core == 0)
+    def _():
+        bytes_of(packs.at[pl.ds(0, n_sp)], a_s.at[0])
+        spare.wait_send()
+
+    @pl.when(core == 1)
+    def _():
+        bytes_of(packs.at[pl.ds(0, n_sp - 1)], a_s.at[0])
+        bytes_of(sendb.at[pl.ds(0, n_dp - 1)], b_s.at[0])
+        for o in range(1, n_tp):
+            bytes_of(sendb, b_s.at[o])
+        bytes_of(cxb, c_s.at[0])
+        bytes_of(cxb.at[pl.ds(1, n_sp - 1)], c_s.at[1])
 
     @pl.when(sp < n_sp - 1)
     def _():
@@ -480,33 +546,34 @@
     act_rows = -(-(samples + 1) // 8) * 8
     pack_rows = -(-(3 * samples + 2) // 8) * 8
     row_table, col_table = rotary_tables(n_sp * tok // GRID_W)
+    table = np.concatenate([col_table, row_table], axis=1)
     vm = pltpu.VMEM
     dma = pltpu.SemaphoreType.DMA
     group = n_dp * cols
     scratch = [
         vm((tok, width), BF16), vm((samples, depth), BF16), vm((depth,), BF16),
-        vm((3, depth, cols), BF16), vm((n_ctx, width), BF16), vm((width, q_width + LANES), BF16),
+        vm((3, depth, cols), BF16), vm((2, n_ctx, width), BF16), vm((width, q_width + LANES), BF16),
         vm(out_weight.shape, BF16), pltpu.SMEM((heads,), F32), pltpu.SMEM((heads,), F32),
-        vm(row_table.shape, F32), vm(col_table.shape, F32),
+        vm(table.shape, F32),
         vm((act_rows, depth), F32), vm((pack_rows, cols), F32), vm((pack_rows, cols), BF16),
-        vm((n_sp - 1, pack_rows, cols), BF16), vm((pack_rows, cols), F32),
-        vm((n_dp, 8, cols), BF16), vm((n_td, 8, cols), BF16), vm((n_tp, 8, group), F32),
-        vm((n_tp, tok, group), F32), vm((n_tp, n_ctx, group), F32), vm((tok, group), BF16),
-        vm((n_ctx, group), BF16), vm((LANES, width), BF16), vm((tok, LANES), F32),
-        vm((tok, LANES), F32), vm((tok, q_width + LANES), F32), vm((n_ctx, LANES), F32),
-        vm((window, LANES), BF16), vm((n_sp, n_ctx, LANES), BF16),
+        vm((2 * n_sp - 1, pack_rows, cols), BF16), vm((2, pack_rows, cols), F32),
+        vm((n_dp, 2, 8, cols), BF16), vm((n_tp, n_dp // 2, 2, 8, cols), BF16),
+        vm((n_tp, 8, group), F32),
+        vm((n_tp, tok, group), F32), vm((n_tp, 2 * n_ctx, group), F32), vm((tok, group), BF16),
+        vm((2 * n_ctx, group), BF16), vm((LANES, width), BF16), vm((tok, LANES), F32),
+        vm((tok, LANES), F32), vm((tok, q_width + LANES), F32), vm((2 * n_ctx, LANES), F32),
+        vm((window, LANES), BF16), vm((2, n_ctx, LANES), BF16), vm((n_sp, n_ctx, LANES), BF16),
         vm((keys, LANES), BF16), vm((keys, LANES), BF16),
         vm((blocks, heads * WINDOW_REACH, LANES), BF16),
         vm((n_tp, blocks, WINDOW_REACH, q_width), BF16),
-        dma((15,)), dma((n_sp - 1,)), dma((n_sp - 1,)), dma((n_td,)),
-        dma((n_td,)), dma((2,)), dma((2,)), dma((n_sp - 1,)), dma((n_sp - 1,)),
-        dma((blocks, n_tp)), dma((blocks, n_tp)),
+        dma((11,)), dma((1,)), dma((1,)), dma((1,)), dma((1,)), dma((n_tp,)), dma((n_tp,)),
+        dma((2,)), dma((2,)), dma((2,)), dma((1,)), dma((2,)), dma((blocks, 2)),
     ]
     stays = pl.BlockSpec(memory_space=pltpu.HBM)
     out = pl.pallas_call(
         functools.partial(block_kernel, (n_sp, n_tp, n_dp, samples)),
         out_shape=pltpu.VMEM((tok, out_cols), F32),
-        in_specs=[stays] * 13,
+        in_specs=[stays] * 12,
         out_specs=pl.BlockSpec(memory_space=pltpu.VMEM),
         scratch_shapes=scratch,
         compiler_params=pltpu.CompilerParams(
@@ -516,7 +583,7 @@
     )(
         latent[0], conditioning, context_cond, modulation, context[0], query_weight,
         key_projection.T, value_projection.T, out_weight, sink_head_logit, prefix_logit_bias,
-        jnp.asarray(row_table), jnp.asarray(col_table),
+        jnp.asarray(table),
     )
     return out[None]
 

time: 28.3 us -> 27 us (0.954)
  Pallas kernels: 27.3 us -> 25.9 us
    pallas_call x1, Pallas kernels: 27.3 us -> 25.9 us  [per_device(): pl.pallas_call(functools.partial(block_kernel, (n_sp, n_tp, n_dp, samples...]
where the time goes in v4:
time: 27 us; the launch traced here: 26.8 us
  Pallas kernels  25.9 us (96%)
  local copies, waits for them, and re-layouts  0.88 us (3%)
    pallas_call x1, Pallas kernels, per_device(): pl.pallas_call(functools.partial(block_kernel, (n_sp, n_tp, n_dp, samples...  25.9 us
    unnamed x1, local copies, waits for them, and re-layouts  0.88 us

profile of v4, /device:TPU:0, one launch (start us, length us, event | category | flops | bytes accessed | tf_op | source)
XLA Modules:
  0.0 26.8 jit_solution(1124826402869664557)
XLA Ops:
  0.0 25.9 %fused_block.1 = f32[384,512]{1,0:T(8,128)S(1)} custom-call(bf16[384,2048]{1,0:T(8,128)(2,1)} %bitcast.6, bf16[2,512]{1,0:T(2,128)(2,1)} %cond_hbm.1, bf16[512]{0:T(512)(128)(2,1)} %cctx_hbm.1, bf16[3,512,256]{2,1,0:T(8,128)(2,1)} %mod_hbm.1, bf16[64,2048]{1,0:T(8,128)(2,1)} %bitcast.7, bf16[2048,256]{1,0:T(8,128)(2,1)} %qw_hbm.1, bf16[64,2048]{1,0:T(8,128)(2,1)} %bitcast.8, ...), custom_call_target="tpu_custom_call" | custom-call | tf_op jit(solution)/shard_map/fused_block/pallas_call | solution.py:573
  25.9 0.9 %copy.14 = f32[1,384,512]{2,1,0:T(8,128)} copy(f32[1,384,512]{2,1,0:T(8,128)S(1)} %bitcast.5) | data formatting | bytes 1572864

commit v5 on v4

--- a/solution.py
+++ b/solution.py
@@ -44,9 +44,9 @@
     sink_hbm, bias_hbm, turn_hbm,
     outv,
     lat, cond, cctx, mod, ctx, wall, ow, sink, bias, angles,
-    act, packf, pack, packs, total, sendb, slots, modv,
+    act, packf, pack, packs, total, sendb, slots, modv, gatef, gates, gateb, gatev,
     xn, xnc, nrm, nrmc, kvw, cosv, sinv, acc, accc, kvb, cxs, cxb, kd, vd, q4, att,
-    in_sem, a_s, a_r, x_s, x_r, b_s, b_r, h_s, h_r, c_s, c_r, g_s, g_r,
+    in_sem, a_s, a_r, x_s, x_r, b_s, b_r, h_s, h_r, c_s, c_r, g_s, g_r, v_s, v_r, w_s, w_r,
 ):
     n_sp, n_tp, n_dp, samples = dims
     sp, tp, dp = lax.axis_index("sp"), lax.axis_index("tp"), lax.axis_index("dp")
@@ -65,12 +65,15 @@
     heads = 2 * pairs
 
     barrier = pltpu.get_barrier_semaphore()
-    for o in range(1, n_sp):
-        for d in (dp, 2 * pair + 1 - core):
-            pl.semaphore_signal(
-                barrier, inc=1, device_id={"sp": lax.rem(sp + o, n_sp), "dp": d},
-                device_id_type=MESH,
-            )
+    @pl.when(core == 1)
+    def _():
+        for o in range(1, n_sp):
+            for d in (2 * pair, 2 * pair + 1):
+                pl.semaphore_signal(
+                    barrier, inc=1, device_id={"sp": lax.rem(sp + o, n_sp), "dp": d},
+                    device_id_type=MESH,
+                )
+
     for o in range(1, n_td):
         lin = lax.rem(me + o, n_td)
         pl.semaphore_signal(
@@ -93,11 +96,13 @@
         return partner(o) if relayed else lax.rem(tp + n_tp - o, n_tp)
 
     pairs_in = [
-        (cond_hbm, cond, 0), (cctx_hbm, cctx, 1), (mod_hbm, mod, 2), (ctx_hbm, ctx.at[0], 3),
-        (lat_hbm, lat, 4), (kw_hbm, kvw.at[pl.ds(0, HEAD_SIZE)], 5),
-        (vw_hbm, kvw.at[pl.ds(HEAD_SIZE, HEAD_SIZE)], 5), (turn_hbm, angles, 6),
-        (qw_hbm, wall.at[:, pl.ds(0, q_width)], 7), (sink_hbm, sink, 8), (bias_hbm, bias, 9),
-        (ow_hbm, ow, 10),
+        (cond_hbm, cond, 0), (cctx_hbm, cctx, 1),
+        (mod_hbm.at[pl.ds(0, 2)], mod.at[pl.ds(0, 2)], 2), (ctx_hbm, ctx.at[0], 3),
+        (mod_hbm.at[2], mod.at[2], 4), (lat_hbm, lat, 5),
+        (kw_hbm, kvw.at[pl.ds(0, HEAD_SIZE)], 6),
+        (vw_hbm, kvw.at[pl.ds(HEAD_SIZE, HEAD_SIZE)], 6),
+        (qw_hbm, wall.at[:, pl.ds(0, q_width)], 6), (turn_hbm, angles, 7), (sink_hbm, sink, 8),
+        (bias_hbm, bias, 9), (ow_hbm, ow, 10),
     ]
     loads = [pltpu.make_async_copy(src, dst, in_sem.at[i]) for src, dst, i in pairs_in]
     for load in loads[:4]:
@@ -124,13 +129,12 @@
     packf[...] = jnp.zeros_like(packf)
     n_rows = samples + 1
     loads[2].wait()
-    for m in range(3):
-        count = n_rows if m < 2 else samples
+    for m in range(2):
         part = jnp.dot(activated, mod[m], preferred_element_type=F32)
-        packf[m * n_rows : m * n_rows + count, :] = part[0:count, :]
+        packf[m * n_rows : (m + 1) * n_rows, :] = part[0:n_rows, :]
     pack[...] = packf[...].astype(BF16)
 
-    pl.semaphore_wait(barrier, 2 * (n_sp - 1) + n_td - 1)
+    pl.semaphore_wait(barrier, n_sp - 1 + n_td - 1)
     a_copies = [
         remote(
             pack, packs.at[2 * o - 1 + core if o else 0], a_s.at[0], a_r.at[0],
@@ -141,11 +145,27 @@
     for copy in a_copies[1:]:
         copy.start()
     spare = remote(ctx.at[0], ctx.at[1], x_s.at[0], x_r.at[0], dp=lead)
+
+    @pl.when(core == 0)
+    def _():
+        a_copies[0].start()
+
+    loads[4].wait()
+    gatef[...] = jnp.dot(activated, mod[2], preferred_element_type=F32)
+    v_copies = [
+        remote(
+            gatef, gates.at[2 * o - 1 + core if o else 0], v_s.at[0], v_r.at[0],
+            sp=lax.rem(sp + o, n_sp), dp=lead,
+        )
+        for o in range(n_sp)
+    ]
+    for copy in v_copies[1:]:
+        copy.start()
     loads[3].wait()
 
     @pl.when(core == 0)
     def _():
-        a_copies[0].start()
+        v_copies[0].start()
         spare.start()
 
     chunk = 64
@@ -173,7 +193,7 @@
             for t in range(n_tp):
                 xnc[t, at : at + chunk, :] = x[:, t * group : (t + 1) * group]
 
-    loads[4].wait()
+    loads[5].wait()
     normalise(lat, xn, 0, tok // chunk)
 
     @pl.when(core == 1)
@@ -185,7 +205,7 @@
 
     b_copies = [
         remote(
-            sendb.at[lax.rem(dp + e, n_dp)], slots.at[o, pair], b_s.at[o], b_r.at[o],
+            sendb.at[lax.rem(dp + e, n_dp)], slots.at[o, pair], b_s.at[0], b_r.at[o],
             tp=partner(o), dp=lax.rem(dp + e, n_dp),
         )
         for o in range(n_tp)
@@ -205,16 +225,16 @@
             for c in range(2):
                 rows = [
                     total[c, source : source + 1, :]
-                    for source in (d, n_rows + d, 2 * n_rows + d, samples, n_rows + samples)
+                    for source in (d, n_rows + d, samples, n_rows + samples)
                 ]
-                rows.append(jnp.zeros((3, cols), F32))
+                rows.append(jnp.zeros((4, cols), F32))
                 sendb[d, c] = jnp.concatenate(rows, axis=0).astype(BF16)
         for copy in b_copies:
             copy.start()
         slots[0, pair] = sendb[dp]
 
-    bytes_of(kvw, in_sem.at[5])
-    for load in loads[7:11]:
+    bytes_of(wall, in_sem.at[6])
+    for load in loads[9:12]:
         load.wait()
     groups = tok // GRID_W
     for g in range(groups):
@@ -238,7 +258,7 @@
         for c in range(2):
             c_copies.append(
                 remote(
-                    cxs.at[c], cxb.at[r], c_s.at[c], c_r.at[0],
+                    cxs.at[c], cxb.at[r], c_s.at[0], c_r.at[0],
                     sp=lax.rem(sp + r, n_sp), dp=2 * pair + c,
                 )
             )
@@ -261,7 +281,7 @@
 
         @pl.when(core == 1)
         def _():
-            condition(xnc, nrmc, 2 * n_ctx, o, g, 3, 4)
+            condition(xnc, nrmc, 2 * n_ctx, o, g, 2, 3)
             u = jnp.dot(nrmc[...], wall[weight_rows, q_width:], preferred_element_type=F32)
             if o:
                 u = accc[...] + u
@@ -309,7 +329,7 @@
          sp=lax.rem(sp + 1, n_sp)
     )
     down = remote(
-        kvb.at[pl.ds(reach, reach)], kvb.at[pl.ds(reach + tok, reach)], h_s.at[1], h_r.at[1],
+        kvb.at[pl.ds(reach, reach)], kvb.at[pl.ds(reach + tok, reach)], h_s.at[0], h_r.at[1],
         sp=lax.rem(sp + n_sp - 1, n_sp),
     )
 
@@ -387,64 +407,92 @@
             powers.append(e)
         return tops, masses, weigh(powers, at)
 
-    g_copies = {}
-
-    def beyond(b, state):
+
+    def beyond(b, state, some):
         tops, masses, weighed = state
-        parts_of = [(window, scores(b, window, n_all_ctx))]
+        first, last = some[0] * reach, (some[-1] + 1) * reach
+        q2 = q4[b, first:last, :]
+
+        def scores(at, count):
+            keys = kd[at : at + count, :]
+            return lax.dot_general(q2, keys, nt, preferred_element_type=F32)
+
+        parts_of = [(window, scores(window, n_all_ctx))]
+        edges = []
         if b == 0:
-            parts_of.append((0, scores(b, 0, reach)))
+            edges.append((0, lambda s: jnp.where(delta >= low_edge, s, MASKED)))
         if b == blocks - 1:
-            parts_of.append((reach + tok, scores(b, reach + tok, reach)))
-        fades, powers = [], [[] for _ in parts_of]
-        for h in range(heads):
-            groups = [[s + bias[h] for s in tiles(parts_of[0][1], h)]]
-            if b == 0:
-                groups.append([jnp.where(delta >= low_edge, parts_of[-1][1][h * reach : (h + 1) * reach], MASKED)])
-            if b == blocks - 1:
-                groups.append([jnp.where(delta <= high_edge, parts_of[-1][1][h * reach : (h + 1) * reach], MASKED)])
+            edges.append((reach + tok, lambda s: jnp.where(delta <= high_edge, s, MASKED)))
+        for at, _ in edges:
+            parts_of.append((at, scores(at, reach)))
+        fades, powers = {}, [[] for _ in parts_of]
+        for i, h in enumerate(some):
+            groups = [[s + bias[h] for s in tiles(parts_of[0][1], i)]]
+            for (_, mask), (_, s) in zip(edges, parts_of[1:]):
+                groups.append([mask(s) for s in tiles(s, i)])
             top = jnp.maximum(top_of(sum(groups, [])), tops[h])
             fade = jnp.exp(tops[h] - top)
             mass = masses[h] * fade
-            for i, parts in enumerate(groups):
+            for kept, parts in zip(powers, groups):
                 e, more = soften(parts, top)
-                powers[i].append(e)
+                kept.append(e)
                 mass = mass + more
             share = 1.0 / mass
-            fades.append((fade * share, share))
+            fades[h] = (fade * share, share)
         more = weigh(powers[0], window)
-        for i in range(1, len(parts_of)):
-            more = more + weigh(powers[i], parts_of[i][0])
+        for kept, (at, _) in zip(powers[1:], parts_of[1:]):
+            more = more + weigh(kept, at)
         low = low_half((reach, LANES))
-        for p in range(pairs):
+        for p in range(some[0] // 2, some[-1] // 2 + 1):
             halves = []
             for h in (2 * p, 2 * p + 1):
                 rows = slice(h * reach, (h + 1) * reach)
-                halves.append(weighed[rows, :] * fades[h][0] + more[rows, :] * fades[h][1])
+                mine = slice(h * reach - first, (h + 1) * reach - first)
+                halves.append(weighed[rows, :] * fades[h][0] + more[mine, :] * fades[h][1])
             att[0, b, :, p * LANES : (p + 1) * LANES] = jnp.where(low, *halves).astype(BF16)
+        lanes = pl.ds(some[0] * HEAD_SIZE, len(some) * HEAD_SIZE)
         for o in direct:
-            g_copies[b, o] = remote(
-                att.at[0, b], att.at[o, b], g_s.at[0], g_r.at[b, 0], tp=partner(o)
-            )
-            g_copies[b, o].start()
+            remote(
+                att.at[0, b, :, lanes], att.at[o, b, :, lanes], g_s.at[0], g_r.at[b, 0],
+                tp=partner(o),
+            ).start()
 
     def forward(b):
         for o in direct:
             part = pl.ds((o - 1) * (reach // 2), reach // 2)
-            g_copies[b, 2 + o] = remote(
-                att.at[o, b, part], att.at[3, b, part], g_s.at[1], g_r.at[b, 1],
-                tp=partner(3 - o),
-            )
-            g_copies[b, 2 + o].start()
+            remote(
+                att.at[o, b, part], att.at[3, b, part], g_s.at[0], g_r.at[b, 1], tp=partner(3 - o)
+            ).start()
 
     order = list(range(1, blocks - 1)) + ([0, blocks - 1] if blocks > 1 else [0])
     states = {}
     for b in order:
         states[b] = within(b)
+    w_copies = [
+        remote(
+            gateb.at[lax.rem(dp + e, n_dp)], gatev.at[pair], w_s.at[0], w_r.at[0],
+            dp=lax.rem(dp + e, n_dp),
+        )
+        for e in range(1, n_dp)
+    ]
+
+    @pl.when(core == 1)
+    def _():
+        bytes_of(gates, v_r.at[0])
+        for c in range(2):
+            summed = gatef[...] if c else gates[0]
+            for o in range(1, n_sp):
+                summed = summed + gates[2 * o - 1 + c]
+            for d in range(n_dp):
+                gateb[d, c] = jnp.broadcast_to(summed[d : d + 1, :], (8, cols))
+        for copy in w_copies:
+            copy.start()
+        gatev[pair] = gateb[dp]
+
 
     @pl.when(core == 0)
     def _():
-        bytes_of(cxb, c_r.at[0])
+        bytes_of(cxb.at[pl.ds(0, n_sp)], c_r.at[0])
 
     @pl.when(core == 1)
     def _():
@@ -473,12 +521,28 @@
                 kvb[reach + tok : window, :] = jnp.zeros((reach, LANES), BF16)
 
             expand(kvb[reach + tok : window, :].astype(F32), reach + tok)
-        beyond(b, states[b])
-
-    loads[11].wait()
+        if b == order[0]:
+            for p in range(pairs):
+                beyond(b, states[b], (2 * p, 2 * p + 1))
+        else:
+            beyond(b, states[b], tuple(range(heads)))
+
+    loads[12].wait()
     out_cols = ow.shape[1]
     mine = pl.ds(pl.multiple_of(tp * out_cols, out_cols), out_cols)
-    gate = modv[0, 2:3, :]
+
+    @pl.when(core == 0)
+    def _():
+        bytes_of(gatev, w_r.at[0])
+
+    if n_pairs > 1:
+        @pl.when(core == 1)
+        def _():
+            bytes_of(gatev.at[pl.ds(1, n_pairs - 1)], w_r.at[0])
+
+    for d in range(n_dp):
+        modv[0, :, d * cols : (d + 1) * cols] = gatev[d // 2, d % 2]
+    gate = modv[0, 0:1, :]
 
     def project(b, o):
         w = ow[pl.ds(pl.multiple_of(owner(o) * q_width, q_width), q_width), :]
@@ -500,31 +564,31 @@
             mixed = mixed + project(b, 3)
         outv[rows, :] = lat[rows, mine].astype(F32) + gate * mixed
 
-    bytes_of(att.at[pl.ds(1, len(direct))], g_s.at[0])
-    if relayed:
-        bytes_of(att.at[3], g_s.at[1])
+    bytes_of(att.at[pl.ds(1, n_tp - 1)], g_s.at[0])
 
     @pl.when(core == 0)
     def _():
         bytes_of(packs.at[pl.ds(0, n_sp)], a_s.at[0])
+        bytes_of(gates.at[pl.ds(0, n_sp)], v_s.at[0])
         spare.wait_send()
 
     @pl.when(core == 1)
     def _():
         bytes_of(packs.at[pl.ds(0, n_sp - 1)], a_s.at[0])
-        bytes_of(sendb.at[pl.ds(0, n_dp - 1)], b_s.at[0])
-        for o in range(1, n_tp):
-            bytes_of(sendb, b_s.at[o])
+        bytes_of(gates.at[pl.ds(0, n_sp - 1)], v_s.at[0])
+        bytes_of(sendb.at[pl.ds(0, n_td - 1)], b_s.at[0])
+        bytes_of(gateb.at[pl.ds(0, n_dp - 1)], w_s.at[0])
         bytes_of(cxb, c_s.at[0])
-        bytes_of(cxb.at[pl.ds(1, n_sp - 1)], c_s.at[1])
-
-    @pl.when(sp < n_sp - 1)
-    def _():
-        up.wait_send()
-
-    @pl.when(sp > 0)
-    def _():
-        down.wait_send()
+
+    edge = jnp.logical_or(sp == 0, sp == n_sp - 1)
+
+    @pl.when(edge)
+    def _():
+        bytes_of(kvb.at[pl.ds(0, reach)], h_s.at[0])
+
+    @pl.when(jnp.logical_not(edge))
+    def _():
+        bytes_of(kvb.at[pl.ds(0, 2 * reach)], h_s.at[0])
 
 
 def per_device(
@@ -544,7 +608,7 @@
     keys = window + n_sp * n_ctx
     n_td = n_tp * n_dp
     act_rows = -(-(samples + 1) // 8) * 8
-    pack_rows = -(-(3 * samples + 2) // 8) * 8
+    pack_rows = -(-(2 * samples + 2) // 8) * 8
     row_table, col_table = rotary_tables(n_sp * tok // GRID_W)
     table = np.concatenate([col_table, row_table], axis=1)
     vm = pltpu.VMEM
@@ -557,17 +621,20 @@
         vm(table.shape, F32),
         vm((act_rows, depth), F32), vm((pack_rows, cols), F32), vm((pack_rows, cols), BF16),
         vm((2 * n_sp - 1, pack_rows, cols), BF16), vm((2, pack_rows, cols), F32),
-        vm((n_dp, 2, 8, cols), BF16), vm((n_tp, n_dp // 2, 2, 8, cols), BF16),
-        vm((n_tp, 8, group), F32),
+        vm((n_td, 2, 8, cols), BF16), vm((n_tp, n_dp // 2, 2, 8, cols), BF16),
+        vm((n_tp, 8, group), F32), vm((act_rows, cols), F32),
+        vm((2 * n_sp - 1, act_rows, cols), F32), vm((n_dp, 2, 8, cols), F32),
+        vm((n_dp // 2, 2, 8, cols), F32),
         vm((n_tp, tok, group), F32), vm((n_tp, 2 * n_ctx, group), F32), vm((tok, group), BF16),
         vm((2 * n_ctx, group), BF16), vm((LANES, width), BF16), vm((tok, LANES), F32),
         vm((tok, LANES), F32), vm((tok, q_width + LANES), F32), vm((2 * n_ctx, LANES), F32),
-        vm((window, LANES), BF16), vm((2, n_ctx, LANES), BF16), vm((n_sp, n_ctx, LANES), BF16),
+        vm((window, LANES), BF16), vm((2, n_ctx, LANES), BF16), vm((2 * n_sp - 1, n_ctx, LANES), BF16),
         vm((keys, LANES), BF16), vm((keys, LANES), BF16),
         vm((blocks, heads * WINDOW_REACH, LANES), BF16),
         vm((n_tp, blocks, WINDOW_REACH, q_width), BF16),
-        dma((11,)), dma((1,)), dma((1,)), dma((1,)), dma((1,)), dma((n_tp,)), dma((n_tp,)),
-        dma((2,)), dma((2,)), dma((2,)), dma((1,)), dma((2,)), dma((blocks, 2)),
+        dma((11,)), dma((1,)), dma((1,)), dma((1,)), dma((1,)), dma((1,)), dma((n_tp,)),
+        dma((1,)), dma((2,)), dma((1,)), dma((1,)), dma((1,)), dma((blocks, 2)), dma((1,)),
+        dma((1,)), dma((1,)), dma((1,)),
     ]
     stays = pl.BlockSpec(memory_space=pltpu.HBM)
     out = pl.pallas_call(

time: 27 us -> 26.4 us (0.978)
  Pallas kernels: 25.9 us -> 25.3 us
    pallas_call x1, Pallas kernels: 25.9 us -> 25.3 us  [per_device(): pl.pallas_call(functools.partial(block_kernel, (n_sp, n_tp, n_dp, samples...]
where the time goes in v5:
time: 26.4 us; the launch traced here: 26.2 us
  Pallas kernels  25.3 us (96%)
  local copies, waits for them, and re-layouts  0.88 us (3%)
    pallas_call x1, Pallas kernels, per_device(): pl.pallas_call(functools.partial(block_kernel, (n_sp, n_tp, n_dp, samples...  25.3 us
    unnamed x1, local copies, waits for them, and re-layouts  0.88 us

profile of v5, /device:TPU:0, one launch (start us, length us, event | category | flops | bytes accessed | tf_op | source)
XLA Modules:
  0.0 26.2 jit_solution(11620102479498275350)
XLA Ops:
  0.0 25.3 %fused_block.1 = f32[384,512]{1,0:T(8,128)S(1)} custom-call(bf16[384,2048]{1,0:T(8,128)(2,1)} %bitcast.6, bf16[2,512]{1,0:T(2,128)(2,1)} %cond_hbm.1, bf16[512]{0:T(512)(128)(2,1)} %cctx_hbm.1, bf16[3,512,256]{2,1,0:T(8,128)(2,1)} %mod_hbm.1, bf16[64,2048]{1,0:T(8,128)(2,1)} %bitcast.7, bf16[2048,256]{1,0:T(8,128)(2,1)} %qw_hbm.1, bf16[64,2048]{1,0:T(8,128)(2,1)} %bitcast.8, ...), custom_call_target="tpu_custom_call" | custom-call | tf_op jit(solution)/shard_map/fused_block/pallas_call | solution.py:640
  25.3 0.9 %copy.14 = f32[1,384,512]{2,1,0:T(8,128)} copy(f32[1,384,512]{2,1,0:T(8,128)S(1)} %bitcast.5) | data formatting | bytes 1572864

commit v6 on v5

--- a/solution.py
+++ b/solution.py
@@ -251,7 +251,7 @@
         shift = modv[o, shift_row : shift_row + 1, :]
         for i in range(0, count, chunk):
             rows = slice(i, i + chunk)
-            dst[rows, :] = (src[g, rows, :] * scale + shift).astype(BF16)
+            dst[o, rows, :] = (src[g, rows, :] * scale + shift).astype(BF16)
 
     c_copies = [remote(cxs.at[0], cxb.at[0], c_s.at[0], c_r.at[0], dp=dp - core)]
     for r in range(1, n_sp):
@@ -262,7 +262,7 @@
                     sp=lax.rem(sp + r, n_sp), dp=2 * pair + c,
                 )
             )
-    for o in range(n_tp):
+    def land(o):
         if o:
             bytes_of(slots.at[o], b_r.at[o])
         else:
@@ -276,29 +276,47 @@
                     bytes_of(slots.at[0, pl.ds(1, n_pairs - 1)], b_r.at[0])
         for d in range(n_dp):
             modv[o, :, d * cols : (d + 1) * cols] = slots[o, d // 2, d % 2].astype(F32)
-        g = owner(o)
-        weight_rows = pl.ds(pl.multiple_of(g * group, group), group)
-
-        @pl.when(core == 1)
-        def _():
-            condition(xnc, nrmc, 2 * n_ctx, o, g, 2, 3)
-            u = jnp.dot(nrmc[...], wall[weight_rows, q_width:], preferred_element_type=F32)
-            if o:
-                u = accc[...] + u
-            if o < n_tp - 1:
-                accc[...] = u
-            else:
-                cxs[0] = u[n_ctx:, :].astype(BF16)
-                cxs[1] = u[0:n_ctx, :].astype(BF16)
-                for copy in c_copies[1:] + c_copies[:1]:
-                    copy.start()
-                cxb[0] = u[0:n_ctx, :].astype(BF16)
-
-        condition(xn, nrm, tok, o, g, 0, 1)
-        u = jnp.dot(nrm[...], wall[weight_rows, :], preferred_element_type=F32)
-        if o:
-            u = acc[...] + u
-        acc[...] = u
+
+    def weight_rows(o):
+        return pl.ds(pl.multiple_of(owner(o) * group, group), group)
+
+    def context_part(o):
+        condition(xnc, nrmc, 2 * n_ctx, o, owner(o), 2, 3)
+        weights = wall[weight_rows(o), q_width:]
+        return jnp.dot(nrmc[o], weights, preferred_element_type=F32)
+
+    def latent_part(o):
+        condition(xn, nrm, tok, o, owner(o), 0, 1)
+        u = jnp.dot(nrm[o], wall[weight_rows(o), :], preferred_element_type=F32)
+        acc[...] = acc[...] + u if o else u
+
+    land(0)
+
+    @pl.when(core == 1)
+    def _():
+        accc[...] = context_part(0)
+
+    latent_part(0)
+
+    @pl.when(core == 1)
+    def _():
+        u = accc[...]
+        for o in range(1, n_tp):
+            land(o)
+            u = u + context_part(o)
+        cxs[0] = u[n_ctx:, :].astype(BF16)
+        cxs[1] = u[0:n_ctx, :].astype(BF16)
+        for copy in c_copies[1:] + c_copies[:1]:
+            copy.start()
+        cxb[0] = u[0:n_ctx, :].astype(BF16)
+        for o in range(1, n_tp):
+            latent_part(o)
+
+    @pl.when(core == 0)
+    def _():
+        for o in range(1, n_tp):
+            land(o)
+            latent_part(o)
 
     half = HEAD_SIZE // 2
     quarter = half // 2
@@ -450,23 +468,32 @@
                 mine = slice(h * reach - first, (h + 1) * reach - first)
                 halves.append(weighed[rows, :] * fades[h][0] + more[mine, :] * fades[h][1])
             att[0, b, :, p * LANES : (p + 1) * LANES] = jnp.where(low, *halves).astype(BF16)
-        lanes = pl.ds(some[0] * HEAD_SIZE, len(some) * HEAD_SIZE)
+
+    middle = reach // 2
+
+    def send(b, o, relay, first=0, count=q_width):
+        if relayed:
+            at = (o - 1) * middle if relay else (2 - o) * middle
+            span = (b, pl.ds(at, middle), pl.ds(first, count))
+        else:
+            span = (b, slice(None), pl.ds(first, count))
+        remote(
+            att.at[(0, *span)], att.at[(o, *span)], g_s.at[0], g_r.at[b, 0 if relay else 1],
+            tp=partner(o),
+        ).start()
+
+    def forward(b):
+        bytes_of(att.at[1, b], g_r.at[b, 0])
         for o in direct:
+            part = pl.ds((o - 1) * middle, middle)
             remote(
-                att.at[0, b, :, lanes], att.at[o, b, :, lanes], g_s.at[0], g_r.at[b, 0],
-                tp=partner(o),
-            ).start()
-
-    def forward(b):
-        for o in direct:
-            part = pl.ds((o - 1) * (reach // 2), reach // 2)
-            remote(
-                att.at[o, b, part], att.at[3, b, part], g_s.at[0], g_r.at[b, 1], tp=partner(3 - o)
+                att.at[o, b, part], att.at[3, b, part], g_s.at[0], g_r.at[b, 2], tp=partner(3 - o)
             ).start()
 
     order = list(range(1, blocks - 1)) + ([0, blocks - 1] if blocks > 1 else [0])
     states = {}
-    for b in order:
+    early = order[: max(len(order) - 1, 1)]
+    for b in early:
         states[b] = within(b)
     w_copies = [
         remote(
@@ -500,7 +527,10 @@
 
     for r in range(n_sp):
         expand(cxb[r].astype(F32), window + r * n_ctx)
+    held = []
     for b in order:
+        if b not in states:
+            states[b] = within(b)
         if b == 0:
             @pl.when(sp > 0)
             def _():
@@ -524,8 +554,19 @@
         if b == order[0]:
             for p in range(pairs):
                 beyond(b, states[b], (2 * p, 2 * p + 1))
+                for o in direct:
+                    send(b, o, True, p * LANES, LANES)
         else:
             beyond(b, states[b], tuple(range(heads)))
+            for o in direct:
+                send(b, o, True)
+        if relayed:
+            held.append(b)
+            if b == order[0] or b == order[-1]:
+                for c in held:
+                    for o in direct:
+                        send(c, o, False)
+                held.clear()
 
     loads[12].wait()
     out_cols = ow.shape[1]
@@ -549,18 +590,24 @@
         return jnp.dot(att[o, b], w, preferred_element_type=F32)
 
     for b in order:
-        bytes_of(att.at[pl.ds(1, len(direct)), b], g_r.at[b, 0])
         if relayed:
             forward(b)
-        mixed = project(b, 0)
+        else:
+            bytes_of(att.at[pl.ds(1, n_tp - 1), b], g_r.at[b, 0])
+        outv[b * reach : (b + 1) * reach, :] = project(b, 0)
+    for b in order:
+        if relayed:
+            bytes_of(att.at[1, b], g_r.at[b, 1])
+        rows = slice(b * reach, (b + 1) * reach)
+        mixed = outv[rows, :]
         for o in direct:
             mixed = mixed + project(b, o)
-        outv[b * reach : (b + 1) * reach, :] = mixed
+        outv[rows, :] = mixed
     for b in order:
         rows = slice(b * reach, (b + 1) * reach)
         mixed = outv[rows, :]
         if relayed:
-            bytes_of(att.at[3, b], g_r.at[b, 1])
+            bytes_of(att.at[3, b], g_r.at[b, 2])
             mixed = mixed + project(b, 3)
         outv[rows, :] = lat[rows, mine].astype(F32) + gate * mixed
 
@@ -625,15 +672,15 @@
         vm((n_tp, 8, group), F32), vm((act_rows, cols), F32),
         vm((2 * n_sp - 1, act_rows, cols), F32), vm((n_dp, 2, 8, cols), F32),
         vm((n_dp // 2, 2, 8, cols), F32),
-        vm((n_tp, tok, group), F32), vm((n_tp, 2 * n_ctx, group), F32), vm((tok, group), BF16),
-        vm((2 * n_ctx, group), BF16), vm((LANES, width), BF16), vm((tok, LANES), F32),
+        vm((n_tp, tok, group), F32), vm((n_tp, 2 * n_ctx, group), F32), vm((n_tp, tok, group), BF16),
+        vm((n_tp, 2 * n_ctx, group), BF16), vm((LANES, width), BF16), vm((tok, LANES), F32),
         vm((tok, LANES), F32), vm((tok, q_width + LANES), F32), vm((2 * n_ctx, LANES), F32),
         vm((window, LANES), BF16), vm((2, n_ctx, LANES), BF16), vm((2 * n_sp - 1, n_ctx, LANES), BF16),
         vm((keys, LANES), BF16), vm((keys, LANES), BF16),
         vm((blocks, heads * WINDOW_REACH, LANES), BF16),
         vm((n_tp, blocks, WINDOW_REACH, q_width), BF16),
         dma((11,)), dma((1,)), dma((1,)), dma((1,)), dma((1,)), dma((1,)), dma((n_tp,)),
-        dma((1,)), dma((2,)), dma((1,)), dma((1,)), dma((1,)), dma((blocks, 2)), dma((1,)),
+        dma((1,)), dma((2,)), dma((1,)), dma((1,)), dma((1,)), dma((blocks, 3)), dma((1,)),
         dma((1,)), dma((1,)), dma((1,)),
     ]
     stays = pl.BlockSpec(memory_space=pltpu.HBM)

time: 26.4 us -> 25.1 us (0.951)
  Pallas kernels: 25.3 us -> 24.1 us
    pallas_call x1, Pallas kernels: 25.3 us -> 24.1 us  [per_device(): pl.pallas_call(functools.partial(block_kernel, (n_sp, n_tp, n_dp, samples...]
where the time goes in v6:
time: 25.1 us; the launch traced here: 25 us
  Pallas kernels  24.1 us (96%)
  local copies, waits for them, and re-layouts  0.88 us (4%)
    pallas_call x1, Pallas kernels, per_device(): pl.pallas_call(functools.partial(block_kernel, (n_sp, n_tp, n_dp, samples...  24.1 us
    unnamed x1, local copies, waits for them, and re-layouts  0.88 us

profile of v6, /device:TPU:0, one launch (start us, length us, event | category | flops | bytes accessed | tf_op | source)
XLA Modules:
  0.0 25.0 jit_solution(302992533654465919)
XLA Ops:
  0.0 24.1 %fused_block.1 = f32[384,512]{1,0:T(8,128)S(1)} custom-call(bf16[384,2048]{1,0:T(8,128)(2,1)} %bitcast.6, bf16[2,512]{1,0:T(2,128)(2,1)} %cond_hbm.1, bf16[512]{0:T(512)(128)(2,1)} %cctx_hbm.1, bf16[3,512,256]{2,1,0:T(8,128)(2,1)} %mod_hbm.1, bf16[64,2048]{1,0:T(8,128)(2,1)} %bitcast.7, bf16[2048,256]{1,0:T(8,128)(2,1)} %qw_hbm.1, bf16[64,2048]{1,0:T(8,128)(2,1)} %bitcast.8, ...), custom_call_target="tpu_custom_call" | custom-call | tf_op jit(solution)/shard_map/fused_block/pallas_call | solution.py:687
  24.1 0.9 %copy.14 = f32[1,384,512]{2,1,0:T(8,128)} copy(f32[1,384,512]{2,1,0:T(8,128)S(1)} %bitcast.5) | data formatting | bytes 1572864

commit v7 on v6

--- a/solution.py
+++ b/solution.py
@@ -44,9 +44,9 @@
     sink_hbm, bias_hbm, turn_hbm,
     outv,
     lat, cond, cctx, mod, ctx, wall, ow, sink, bias, angles,
-    act, packf, pack, packs, total, sendb, slots, modv, gatef, gates, gateb, gatev,
+    act, packf, pack, packs, sendb, slots, modv, gatef, gates, gateb, gatev,
     xn, xnc, nrm, nrmc, kvw, cosv, sinv, acc, accc, kvb, cxs, cxb, kd, vd, q4, att,
-    in_sem, a_s, a_r, x_s, x_r, b_s, b_r, h_s, h_r, c_s, c_r, g_s, g_r, v_s, v_r, w_s, w_r,
+    a_r, x_r, b_r, h_r, c_r, g_r, v_r, w_r, in_sem, a_s, x_s, b_s, h_s, c_s, g_s, v_s, w_s,
 ):
     n_sp, n_tp, n_dp, samples = dims
     sp, tp, dp = lax.axis_index("sp"), lax.axis_index("tp"), lax.axis_index("dp")
@@ -120,18 +120,20 @@
     act[...] = jnp.zeros_like(act)
     loads[0].wait()
     loads[1].wait()
-    for load in loads[4:]:
-        load.start()
     act[0:samples, :] = cond[...].astype(F32)
     act[samples : samples + 1, :] = cctx[...].astype(F32).reshape(1, cctx.shape[0])
     v = act[...]
     activated = (v / (1.0 + jnp.exp(-v))).astype(BF16)
-    packf[...] = jnp.zeros_like(packf)
-    n_rows = samples + 1
+    for load in loads[4:]:
+        load.start()
     loads[2].wait()
-    for m in range(2):
-        part = jnp.dot(activated, mod[m], preferred_element_type=F32)
-        packf[m * n_rows : (m + 1) * n_rows, :] = part[0:n_rows, :]
+    shift = jnp.dot(activated, mod[0], preferred_element_type=F32)
+    scale = jnp.dot(activated, mod[1], preferred_element_type=F32)
+    rows = [
+        part[r : r + 1, :] for d in range(samples) for r in (d, samples) for part in (shift, scale)
+    ]
+    rows += [jnp.zeros_like(rows[0])] * (packf.shape[0] - len(rows))
+    packf[...] = jnp.concatenate(rows, axis=0)
     pack[...] = packf[...].astype(BF16)
 
     pl.semaphore_wait(barrier, n_sp - 1 + n_td - 1)
@@ -142,7 +144,7 @@
         )
         for o in range(n_sp)
     ]
-    for copy in a_copies[1:]:
+    for copy in a_copies[:0:-1]:
         copy.start()
     spare = remote(ctx.at[0], ctx.at[1], x_s.at[0], x_r.at[0], dp=lead)
 
@@ -208,7 +210,7 @@
             sendb.at[lax.rem(dp + e, n_dp)], slots.at[o, pair], b_s.at[0], b_r.at[o],
             tp=partner(o), dp=lax.rem(dp + e, n_dp),
         )
-        for o in range(n_tp)
+        for o in reversed(range(n_tp))
         for e in range(n_dp)
         if o or e
     ]
@@ -220,15 +222,8 @@
             summed = packf[...] if c else packs[0].astype(F32)
             for o in range(1, n_sp):
                 summed = summed + packs[2 * o - 1 + c].astype(F32)
-            total[c] = summed
-        for d in range(n_dp):
-            for c in range(2):
-                rows = [
-                    total[c, source : source + 1, :]
-                    for source in (d, n_rows + d, samples, n_rows + samples)
-                ]
-                rows.append(jnp.zeros((4, cols), F32))
-                sendb[d, c] = jnp.concatenate(rows, axis=0).astype(BF16)
+            for d in range(n_dp):
+                sendb[d, c] = summed[4 * d : 4 * d + 4, :].astype(BF16)
         for copy in b_copies:
             copy.start()
         slots[0, pair] = sendb[dp]
@@ -275,7 +270,7 @@
                 def _():
                     bytes_of(slots.at[0, pl.ds(1, n_pairs - 1)], b_r.at[0])
         for d in range(n_dp):
-            modv[o, :, d * cols : (d + 1) * cols] = slots[o, d // 2, d % 2].astype(F32)
+            modv[o, 0:4, d * cols : (d + 1) * cols] = slots[o, d // 2, d % 2].astype(F32)
 
     def weight_rows(o):
         return pl.ds(pl.multiple_of(owner(o) * group, group), group)
@@ -492,7 +487,7 @@
 
     order = list(range(1, blocks - 1)) + ([0, blocks - 1] if blocks > 1 else [0])
     states = {}
-    early = order[: max(len(order) - 1, 1)]
+    early = order
     for b in early:
         states[b] = within(b)
     w_copies = [
@@ -638,6 +633,13 @@
         bytes_of(kvb.at[pl.ds(0, 2 * reach)], h_s.at[0])
 
 
+def scoped_kernel(dims, *refs):
+    dma = pltpu.SemaphoreType.DMA
+    pl.run_scoped(
+        lambda *local: block_kernel(dims, *refs, *local), dma((11,)), *[dma((1,))] * 8
+    )
+
+
 def per_device(
     latent, conditioning, context_cond, modulation, context, query_weight, key_projection,
     value_projection, out_weight, sink_head_logit, prefix_logit_bias,
@@ -655,7 +657,7 @@
     keys = window + n_sp * n_ctx
     n_td = n_tp * n_dp
     act_rows = -(-(samples + 1) // 8) * 8
-    pack_rows = -(-(2 * samples + 2) // 8) * 8
+    pack_rows = -(-(4 * samples) // 8) * 8
     row_table, col_table = rotary_tables(n_sp * tok // GRID_W)
     table = np.concatenate([col_table, row_table], axis=1)
     vm = pltpu.VMEM
@@ -667,8 +669,8 @@
         vm(out_weight.shape, BF16), pltpu.SMEM((heads,), F32), pltpu.SMEM((heads,), F32),
         vm(table.shape, F32),
         vm((act_rows, depth), F32), vm((pack_rows, cols), F32), vm((pack_rows, cols), BF16),
-        vm((2 * n_sp - 1, pack_rows, cols), BF16), vm((2, pack_rows, cols), F32),
-        vm((n_td, 2, 8, cols), BF16), vm((n_tp, n_dp // 2, 2, 8, cols), BF16),
+        vm((2 * n_sp - 1, pack_rows, cols), BF16),
+        vm((n_td, 2, 4, cols), BF16), vm((n_tp, n_dp // 2, 2, 4, cols), BF16),
         vm((n_tp, 8, group), F32), vm((act_rows, cols), F32),
         vm((2 * n_sp - 1, act_rows, cols), F32), vm((n_dp, 2, 8, cols), F32),
         vm((n_dp // 2, 2, 8, cols), F32),
@@ -679,13 +681,12 @@
         vm((keys, LANES), BF16), vm((keys, LANES), BF16),
         vm((blocks, heads * WINDOW_REACH, LANES), BF16),
         vm((n_tp, blocks, WINDOW_REACH, q_width), BF16),
-        dma((11,)), dma((1,)), dma((1,)), dma((1,)), dma((1,)), dma((1,)), dma((n_tp,)),
-        dma((1,)), dma((2,)), dma((1,)), dma((1,)), dma((1,)), dma((blocks, 3)), dma((1,)),
-        dma((1,)), dma((1,)), dma((1,)),
+        dma((1,)), dma((1,)), dma((n_tp,)), dma((2,)), dma((1,)), dma((blocks, 3)), dma((1,)),
+        dma((1,)),
     ]
     stays = pl.BlockSpec(memory_space=pltpu.HBM)
     out = pl.pallas_call(
-        functools.partial(block_kernel, (n_sp, n_tp, n_dp, samples)),
+        functools.partial(scoped_kernel, (n_sp, n_tp, n_dp, samples)),
         out_shape=pltpu.VMEM((tok, out_cols), F32),
         in_specs=[stays] * 12,
         out_specs=pl.BlockSpec(memory_space=pltpu.VMEM),

time: 25.1 us -> 24.8 us (0.988)
  Pallas kernels: 24.1 us -> 23.7 us
    pallas_call x1, Pallas kernels: 24.1 us -> 23.7 us  [per_device(): pl.pallas_call(functools.partial(scoped_kernel, (n_sp, n_tp, n_dp, sample...]
where the time goes in v7:
time: 24.8 us; the launch traced here: 24.6 us
  Pallas kernels  23.7 us (96%)
  local copies, waits for them, and re-layouts  0.88 us (4%)
    pallas_call x1, Pallas kernels, per_device(): pl.pallas_call(functools.partial(scoped_kernel, (n_sp, n_tp, n_dp, sample...  23.7 us
    unnamed x1, local copies, waits for them, and re-layouts  0.88 us

profile of v7, /device:TPU:0, one launch (start us, length us, event | category | flops | bytes accessed | tf_op | source)
XLA Modules:
  0.0 24.6 jit_solution(657362542004856762)
XLA Ops:
  0.0 23.7 %fused_block.1 = f32[384,512]{1,0:T(8,128)S(1)} custom-call(bf16[384,2048]{1,0:T(8,128)(2,1)} %bitcast.6, bf16[2,512]{1,0:T(2,128)(2,1)} %refs_1_.1, bf16[512]{0:T(512)(128)(2,1)} %refs_2_.1, bf16[3,512,256]{2,1,0:T(8,128)(2,1)} %refs_3_.1, bf16[64,2048]{1,0:T(8,128)(2,1)} %bitcast.7, bf16[2048,256]{1,0:T(8,128)(2,1)} %refs_5_.1, bf16[64,2048]{1,0:T(8,128)(2,1)} %bitcast.8, ...), custom_call_target="tpu_custom_call" | custom-call | tf_op jit(solution)/shard_map/fused_block/pallas_call | solution.py:688
  23.8 0.9 %copy.14 = f32[1,384,512]{2,1,0:T(8,128)} copy(f32[1,384,512]{2,1,0:T(8,128)S(1)} %bitcast.5) | data formatting | bytes 1572864

commit v8 on v7

--- a/solution.py
+++ b/solution.py
@@ -546,15 +546,9 @@
                 kvb[reach + tok : window, :] = jnp.zeros((reach, LANES), BF16)
 
             expand(kvb[reach + tok : window, :].astype(F32), reach + tok)
-        if b == order[0]:
-            for p in range(pairs):
-                beyond(b, states[b], (2 * p, 2 * p + 1))
-                for o in direct:
-                    send(b, o, True, p * LANES, LANES)
-        else:
-            beyond(b, states[b], tuple(range(heads)))
-            for o in direct:
-                send(b, o, True)
+        beyond(b, states[b], tuple(range(heads)))
+        for o in direct:
+            send(b, o, True)
         if relayed:
             held.append(b)
             if b == order[0] or b == order[-1]:

time: 24.8 us -> 24.6 us (level)
  no operation moved by 1% of the time
where the time goes in v8:
time: 24.6 us; the launch traced here: 24.5 us
  Pallas kernels  23.6 us (96%)
  local copies, waits for them, and re-layouts  0.88 us (4%)
    pallas_call x1, Pallas kernels, per_device(): pl.pallas_call(functools.partial(scoped_kernel, (n_sp, n_tp, n_dp, sample...  23.6 us
    unnamed x1, local copies, waits for them, and re-layouts  0.88 us

profile of v8, /device:TPU:0, one launch (start us, length us, event | category | flops | bytes accessed | tf_op | source)
XLA Modules:
  0.0 24.5 jit_solution(9925283692911744447)
XLA Ops:
  0.0 23.6 %fused_block.1 = f32[384,512]{1,0:T(8,128)S(1)} custom-call(bf16[384,2048]{1,0:T(8,128)(2,1)} %bitcast.6, bf16[2,512]{1,0:T(2,128)(2,1)} %refs_1_.1, bf16[512]{0:T(512)(128)(2,1)} %refs_2_.1, bf16[3,512,256]{2,1,0:T(8,128)(2,1)} %refs_3_.1, bf16[64,2048]{1,0:T(8,128)(2,1)} %bitcast.7, bf16[2048,256]{1,0:T(8,128)(2,1)} %refs_5_.1, bf16[64,2048]{1,0:T(8,128)(2,1)} %bitcast.8, ...), custom_call_target="tpu_custom_call" | custom-call | tf_op jit(solution)/shard_map/fused_block/pallas_call | solution.py:682
  23.6 0.9 %copy.14 = f32[1,384,512]{2,1,0:T(8,128)} copy(f32[1,384,512]{2,1,0:T(8,128)S(1)} %bitcast.5) | data formatting | bytes 1572864
